TPU v7x, 128 devices: a whole 4x4x4 slice. The times are simulated.
128 devices in a mesh: ep: 64 (over z, y, x), tp: 2 (over core).
Axes of the slice: x: 4, y: 4, z: 4, core: 2. Of those that a mesh axis runs over, the one named last changes fastest.
Arguments:
- tokens: bfloat16 [1536, 4096], P('ep'), may hold values from -6 to 6
- cotangent: bfloat16 [1536, 4096], P('ep'), may hold values from -6 to 6
- routes: int32 [1536, 2], P('ep'), may hold values from 0 to 7, all different within a row; in each aligned block of 24 rows (0 to 23, 24 to 47, ...) at most 12 rows name the same one
- route_weights: float32 [1536, 2], P('ep'), may hold values from 0.1 to 0.9
- gate_weight: bfloat16 [64, 4096, 688], P('ep', None, 'tp'), may hold values from -0.09375 to 0.09375
- up_weight: bfloat16 [64, 4096, 688], P('ep', None, 'tp'), may hold values from -0.09375 to 0.09375
- down_weight: bfloat16 [64, 688, 4096], P('ep', 'tp'), may hold values from -0.078125 to 0.078125
Outputs:
- token_grad: bfloat16 [1536, 4096], P('ep', 'tp')
- route_grad: float32 [1536, 2], P('ep')
- gate_grad: bfloat16 [64, 4096, 688], P('ep', None, 'tp')
- up_grad: bfloat16 [64, 4096, 688], P('ep', None, 'tp')
- down_grad: bfloat16 [64, 688, 4096], P('ep', 'tp')
Inputs may be any that keep to these rules, and one draw needn't show every extreme that they name: `routes`: each row names 2 different experts of 0 to 7; within the rows of one device (24 aligned rows) no expert is named more than 12 times, and in some blocks one is named exactly 12 times.
All inputs are finite; a program needn't handle non-finite values.
Results may differ from a plain program's by a relative error of at most 0.01.
Values may be sent and summed in bfloat16 or wider, within the bound.
A program may use at most 192 MiB of HBM per device.

v0:
```python
import jax
import jax.numpy as jnp
from jax import lax
from jax.sharding import PartitionSpec as P

EXPERTS = 8
TOP = 2
CAP = 12


def silu_slope(pre_gate):
    sigma = jax.nn.sigmoid(pre_gate)
    return sigma * (1.0 + pre_gate * (1.0 - sigma))


def expert_pass(rows_in, rows_cot, shares, gate_mat, up_mat, down_mat):
    pre_gate = jnp.dot(rows_in, gate_mat, preferred_element_type=jnp.float32)
    pre_up = jnp.dot(rows_in, up_mat, preferred_element_type=jnp.float32)
    active = jax.nn.silu(pre_gate)
    hidden = (active * pre_up).astype(jnp.bfloat16)
    expert_out = jnp.dot(hidden, down_mat, preferred_element_type=jnp.float32)
    share_grad = jnp.sum(rows_cot.astype(jnp.float32) * expert_out, axis=1)
    scaled = (rows_cot.astype(jnp.float32) * shares[:, None]).astype(jnp.bfloat16)
    hidden_grad = lax.dot_general(
        scaled, down_mat, (((1,), (1,)), ((), ())), preferred_element_type=jnp.float32
    )
    gate_side = (hidden_grad * pre_up * silu_slope(pre_gate)).astype(jnp.bfloat16)
    up_side = (hidden_grad * active).astype(jnp.bfloat16)
    down_grad = lax.dot_general(
        hidden, scaled, (((0,), (0,)), ((), ())), preferred_element_type=jnp.float32
    ).astype(jnp.bfloat16)
    gate_grad = lax.dot_general(
        rows_in, gate_side, (((0,), (0,)), ((), ())), preferred_element_type=jnp.float32
    ).astype(jnp.bfloat16)
    up_grad = lax.dot_general(
        rows_in, up_side, (((0,), (0,)), ((), ())), preferred_element_type=jnp.float32
    ).astype(jnp.bfloat16)
    token_part = lax.dot_general(
        gate_side, gate_mat, (((1,), (1,)), ((), ())), preferred_element_type=jnp.float32
    )
    token_part = token_part + lax.dot_general(
        up_side, up_mat, (((1,), (1,)), ((), ())), preferred_element_type=jnp.float32
    )
    return (gate_grad, up_grad, down_grad, token_part, share_grad)


def per_device(tokens, cotangent, routes, route_weights, gate_weight, up_weight, down_weight):
    ep_count = lax.axis_size("ep")
    core_count = lax.axis_size("tp")
    span = ep_count // EXPERTS
    slots = EXPERTS * CAP
    width = tokens.shape[1]
    flat_routes = routes.reshape(-1)
    expert_hot = (flat_routes[:, None] == jnp.arange(EXPERTS, dtype=jnp.int32)[None, :]).astype(
        jnp.int32
    )
    before = jnp.cumsum(expert_hot, axis=0) - expert_hot
    position = jnp.sum(before * expert_hot, axis=1)
    slot_of = flat_routes * CAP + position
    placing = jnp.arange(slots, dtype=jnp.int32)[:, None] == slot_of[None, :]
    place_half = placing.astype(jnp.bfloat16)
    place_full = placing.astype(jnp.float32)

    def to_slots(rows):
        paired = jnp.repeat(rows, TOP, axis=0)
        filled = jnp.dot(place_half, paired, preferred_element_type=jnp.float32).astype(
            jnp.bfloat16
        )
        columns = filled.shape[1]
        spread = jnp.broadcast_to(
            filled.reshape(EXPERTS, 1, CAP, columns), (EXPERTS, span, CAP, columns)
        )
        return spread.reshape(ep_count, CAP, columns)

    share_slots = jnp.dot(place_full, route_weights.reshape(-1), precision=lax.Precision.HIGHEST)
    share_send = jnp.broadcast_to(
        share_slots.reshape(EXPERTS, 1, CAP), (EXPERTS, span, CAP)
    ).reshape(ep_count, CAP)
    received_shares = lax.all_to_all(share_send, "ep", split_axis=0, concat_axis=0, tiled=True)
    half_width = width // core_count
    core_index = lax.axis_index("tp")
    token_piece = lax.dynamic_slice_in_dim(tokens, core_index * half_width, half_width, 1)
    cot_piece = lax.dynamic_slice_in_dim(cotangent, core_index * half_width, half_width, 1)
    part_in, part_cot = (
        lax.all_to_all(to_slots(token_piece), "ep", split_axis=0, concat_axis=0, tiled=True),
        lax.all_to_all(to_slots(cot_piece), "ep", split_axis=0, concat_axis=0, tiled=True),
    )
    rows_in, rows_cot = (
        lax.all_gather(part_in, "tp", axis=2, tiled=True),
        lax.all_gather(part_cot, "tp", axis=2, tiled=True),
    )
    total_rows = ep_count * CAP
    gate_grad, up_grad, down_grad, token_terms, share_terms = expert_pass(
        rows_in.reshape(total_rows, width),
        rows_cot.reshape(total_rows, width),
        received_shares.reshape(total_rows),
        gate_weight[0],
        up_weight[0],
        down_weight[0],
    )
    share_spread = jnp.broadcast_to(
        share_terms.reshape(ep_count, CAP, 1), (ep_count, CAP, core_count)
    )
    summed_rows, summed_shares = (
        lax.psum_scatter(
            token_terms.reshape(ep_count, CAP, width).astype(jnp.bfloat16),
            "tp",
            scatter_dimension=2,
            tiled=True,
        ).astype(jnp.float32),
        lax.psum_scatter(
            share_spread.astype(jnp.bfloat16), "tp", scatter_dimension=2, tiled=True
        ).astype(jnp.float32),
    )
    back_rows, back_shares = (
        lax.all_to_all(
            summed_rows.astype(jnp.bfloat16), "ep", split_axis=0, concat_axis=0, tiled=True
        ).astype(summed_rows.dtype),
        lax.all_to_all(
            summed_shares.astype(jnp.bfloat16), "ep", split_axis=0, concat_axis=0, tiled=True
        ).astype(summed_shares.dtype),
    )
    piece_width = back_rows.shape[2]
    slot_rows = jnp.sum(back_rows.reshape(EXPERTS, span, CAP, piece_width), axis=1).reshape(
        slots, piece_width
    )
    slot_shares = jnp.sum(back_shares.reshape(EXPERTS, span, CAP), axis=1).reshape(slots)
    pair_rows = lax.dot_general(
        place_full, slot_rows, (((0,), (0,)), ((), ())), precision=lax.Precision.HIGHEST
    )
    token_grad = jnp.sum(pair_rows.reshape(-1, TOP, piece_width), axis=1).astype(jnp.bfloat16)
    route_grad = lax.dot_general(
        place_full, slot_shares, (((0,), (0,)), ((), ())), precision=lax.Precision.HIGHEST
    ).reshape(-1, TOP)
    return (token_grad, route_grad, gate_grad[None], up_grad[None], down_grad[None])


def solution(mesh):
    return jax.shard_map(
        per_device,
        mesh=mesh,
        in_specs=(
            P("ep", None),
            P("ep", None),
            P("ep", None),
            P("ep", None),
            P("ep", None, "tp"),
            P("ep", None, "tp"),
            P("ep", "tp", None),
        ),
        out_specs=(
            P("ep", "tp"),
            P("ep", None),
            P("ep", None, "tp"),
            P("ep", None, "tp"),
            P("ep", "tp", None),
        ),
        check_vma=False,
    )
```

profile of v0, /device:TPU:0, one launch (start us, length us, event | category | flops | bytes accessed | tf_op | source)
XLA Modules:
  0.0 356.3 jit_solution(2235834668654740104)
XLA Ops:
  10.7 1.1 broadcast_in_dim.43
  12.4 69.3 %all_to_all.29 = bf16[64,12,2048]{2,1,0:T(8,128)(2,1)} all-to-all(bf16[64,12,2048]{2,1,0:T(8,128)(2,1)S(1)} %bitcast.55), channel_id=1, replica_groups=mesh['ep'=64,'tp'=2] {'ep'}, dimensions={0} | all-to-all | bytes 6291456 | tf_op jit(solution)/shard_map/all_to_all | solution.py:86
  84.5 70.4 %all_to_all.30 = bf16[64,12,2048]{2,1,0:T(8,128)(2,1)} all-to-all(bf16[64,12,2048]{2,1,0:T(8,128)(2,1)S(1)} %bitcast.56), channel_id=1, replica_groups=mesh['ep'=64,'tp'=2] {'ep'}, dimensions={0} | all-to-all | bytes 6291456 | tf_op jit(solution)/shard_map/all_to_all | solution.py:85
  156.2 16.5 %all_to_all.31 = f32[64,1,12]{2,1,0:T(1,128)S(1)} all-to-all(f32[64,1,12]{2,1,0:T(1,128)S(1)} %bitcast.60), channel_id=1, replica_groups=mesh['ep'=64,'tp'=2] {'ep'}, dimensions={0} | all-to-all | bytes 6144 | tf_op jit(solution)/shard_map/all_to_all | solution.py:79
  172.7 10.1 %multiply_convert_fusion = bf16[64,12,4096]{2,1,0:T(8,128)(2,1)} fusion(f32[64,12]{1,0:T(8,128)S(1)} %bitcast.59, bf16[64,12,4096]{2,1,0:T(8,128)(2,1)} %all-gather.3.cloned.1.call-done), kind=kLoop, calls=%fused_computation | loop fusion | flops 9437184 | bytes 12585984 | tf_op jit(solution)/shard_map/convert_element_type | solution.py:23
  182.8 9.9 %convert_element_type.73 = bf16[768,4096]{1,0:T(8,128)(2,1)} reshape(bf16[64,12,4096]{2,1,0:T(8,128)(2,1)} %multiply_convert_fusion) | data formatting | bytes 12582912 | tf_op jit(solution)/shard_map/convert_element_type | solution.py:23
  192.7 9.9 %reshape.151 = bf16[768,4096]{1,0:T(8,128)(2,1)} reshape(bf16[64,12,4096]{2,1,0:T(8,128)(2,1)} %all-gather.5.cloned.1.call-done) | data formatting | bytes 12582912 | tf_op jit(solution)/shard_map/reshape | solution.py:94
  202.6 6.2 %fusion.8 = f32[768,344]{0,1:T(8,128)S(1)} fusion(bf16[768,4096]{1,0:T(8,128)(2,1)} %reshape.151, bf16[1,4096,344]{1,2,0:T(8,128)(2,1)} %param.11), kind=kOutput, calls=%fused_computation.15 | convolution fusion | flops 2164260864 | bytes 10166272 | tf_op jit(solution)/shard_map/dot_general | solution.py:17
  208.8 2.5 fusion.14
  211.4 3.7 %multiply_convert_fusion.7 = (bf16[768,344]{0,1:T(8,128)(2,1)S(1)}, bf16[768,344]{0,1:T(8,128)(2,1)}, bf16[768,344]{0,1:T(8,128)(2,1)}) fusion(f32[768,344]{0,1:T(8,128)S(1)} %fusion.8, f32[768,344]{0,1:T(8,128)S(1)} %fusion.14, bf16[768,4096]{1,0:T(8,128)(2,1)S(1)} %bitcast.58, bf16[1,4096,344]{1,2,0:T(8,128)(2,1)S(1)} %copy-done), kind=kOutput, calls=%fused_computation.26 | convolution fusion | flops 2168223744 | bytes 12808192 | tf_op jit(solution)/shard_map/dot_general | solution.py:18
  215.1 11.4 %reshape.160 = f32[768,4096]{1,0:T(8,128)} reshape(bf16[64,12,4096]{2,1,0:T(8,128)(2,1)} %all-gather.3.cloned.1.call-done) | data formatting | bytes 18874368 | tf_op jit(solution)/shard_map/convert_element_type | solution.py:23
  226.4 7.5 %multiply_reduce_fusion = bf16[768]{0:T(1024)(128)(2,1)S(1)} fusion(f32[768,4096]{1,0:T(8,128)} %reshape.160, bf16[768,344]{0,1:T(8,128)(2,1)S(1)} %get-tuple-element.5, bf16[1,344,4096]{2,1,0:T(8,128)(2,1)} %param.13), kind=kOutput, calls=%fused_computation.2 | convolution fusion | flops 2170551552 | bytes 15930880 | tf_op jit(solution)/shard_map/dot_general | solution.py:21
  234.8 5.5 %fusion.6 = f32[768,4096]{1,0:T(8,128)S(1)} fusion(bf16[768,344]{0,1:T(8,128)(2,1)} %get-tuple-element.6, bf16[1,4096,344]{1,2,0:T(8,128)(2,1)} %param.11), kind=kOutput, calls=%fused_computation.13 | convolution fusion | flops 2164260864 | bytes 15929344 | tf_op jit(solution)/shard_map/dot_general | solution.py:38
  240.3 5.6 %add_convert_fusion = bf16[768,4096]{1,0:T(8,128)(2,1)} fusion(f32[768,4096]{1,0:T(8,128)S(1)} %fusion.6, bf16[768,344]{0,1:T(8,128)(2,1)S(1)} %copy-done.3, bf16[1,4096,344]{1,2,0:T(8,128)(2,1)S(1)} %copy-done), kind=kOutput, calls=%fused_computation.3 | convolution fusion | flops 2170552320 | bytes 22220800 | tf_op jit(solution)/shard_map/dot_general | solution.py:41
  246.0 9.7 %convert_element_type.78 = bf16[64,12,4096]{2,1,0:T(8,128)(2,1)} reshape(bf16[768,4096]{1,0:T(8,128)(2,1)} %add_convert_fusion) | data formatting | bytes 12582912 | tf_op jit(solution)/shard_map/convert_element_type | solution.py:106
  256.6 14.4 %all_to_all.32 = bf16[64,12,1]{1,2,0:T(2,128)(2,1)S(1)} all-to-all(bf16[64,12,1]{1,2,0:T(2,128)(2,1)S(1)} %copy.34), channel_id=1, replica_groups=mesh['ep'=64,'tp'=2] {'ep'}, dimensions={0} | all-to-all | bytes 3072 | tf_op jit(solution)/shard_map/all_to_all | solution.py:119
  271.0 10.8 %all-to-all-start.3 = ((bf16[64,12,2048]{2,1,0:T(8,128)(2,1)}), bf16[64,12,2048]{2,1,0:T(8,128)(2,1)}, u32[]{:S(2)}, u32[]{:S(2)}) async-start(bf16[64,12,2048]{2,1,0:T(8,128)(2,1)} %reduce-scatter.3.cloned.1.call-done), calls=%async_computation.4 | async-start | bytes 8388608 | tf_op jit(solution)/shard_map/all_to_all | solution.py:116
  283.3 6.9 %fusion.3 = bf16[1,4096,344]{1,2,0:T(8,128)(2,1)} fusion(bf16[768,4096]{1,0:T(8,128)(2,1)} %reshape.151, bf16[768,344]{0,1:T(8,128)(2,1)} %get-tuple-element.6), kind=kOutput, calls=%fused_computation.10 | convolution fusion | flops 2165669888 | bytes 9637888 | tf_op jit(solution)/shard_map/dot_general | solution.py:32
  290.2 6.9 %fusion.4 = bf16[1,4096,344]{1,2,0:T(8,128)(2,1)} fusion(bf16[768,4096]{1,0:T(8,128)(2,1)} %reshape.151, bf16[768,344]{0,1:T(8,128)(2,1)S(1)} %copy-done.4), kind=kOutput, calls=%fused_computation.11 | convolution fusion | flops 2165669888 | bytes 9637888 | tf_op jit(solution)/shard_map/dot_general | solution.py:35
  297.1 4.1 %fusion.5 = bf16[1,344,4096]{2,1,0:T(8,128)(2,1)} fusion(bf16[768,344]{0,1:T(8,128)(2,1)S(1)} %get-tuple-element.5, f32[768,4096]{1,0:T(8,128)S(1)} %bitcast.54, f32[768]{0:T(1024)S(1)} %mul.74), kind=kOutput, calls=%fused_computation.12 | convolution fusion | flops 2171961344 | bytes 15932416 | tf_op jit(solution)/shard_map/dot_general | solution.py:29
  302.5 38.8 %all-to-all-done.3 = bf16[64,12,2048]{2,1,0:T(8,128)(2,1)} async-done(((bf16[64,12,2048]{2,1,0:T(8,128)(2,1)}), bf16[64,12,2048]{2,1,0:T(8,128)(2,1)}, u32[]{:S(2)}, u32[]{:S(2)}) %all-to-all-start.3) | async-done | bytes 3145760 | tf_op jit(solution)/shard_map/all_to_all | solution.py:116
  341.3 4.0 %convert_reduce_fusion = f32[8,12,2048]{2,1,0:T(8,128)} fusion(bf16[64,12,2048]{2,1,0:T(8,128)(2,1)} %all-to-all-done.3), kind=kLoop, calls=%fused_computation.4 | loop fusion | flops 2949120 | bytes 3932160 | tf_op jit(solution)/shard_map/reduce_sum | solution.py:124
  345.3 2.2 reshape.165
  347.6 2.2 convolution_reduce_fusion
  (73 shorter events, 12.6 us)
Async XLA Ops:
  7.2 204.2 %copy-start = (bf16[1,4096,344]{1,2,0:T(8,128)(2,1)S(1)}, bf16[1,4096,344]{1,2,0:T(8,128)(2,1)}, u32[]{:S(2)}) copy-start(bf16[1,4096,344]{1,2,0:T(8,128)(2,1)} %param.12) | copy-start | bytes 8454148
  7.2 165.6 %all-gather.3.cloned.1.call-start = ((), (), s32[]{:S(2)}) async-start(), calls=%async_computation.7 | async-start | bytes 12582912 | tf_op jit(solution)/shard_map/all_gather | solution.py:90
  81.7 111.0 %all-gather.5.cloned.1.call-start = ((), (), s32[]{:S(2)}) async-start(), calls=%async_computation.8 | async-start | bytes 12582912 | tf_op jit(solution)/shard_map/all_gather | solution.py:89
  154.9 0.7 copy-start.5
  154.9 100.9 %reduce-scatter.5.cloned.1.call-start = ((), (), s32[]{:S(2)}) async-start(), calls=%async_computation.10 | async-start | bytes 12288 | tf_op jit(solution)/shard_map/reduce_scatter | solution.py:111
  202.6 6.2 %copy-start.1 = (bf16[768,4096]{1,0:T(8,128)(2,1)S(1)}, bf16[768,4096]{1,0:T(8,128)(2,1)}, u32[]{:S(2)}) copy-start(bf16[768,4096]{1,0:T(8,128)(2,1)} %convert_element_type.73) | copy-start | bytes 18874372
  202.6 6.2 %copy-start.2 = (bf16[1,344,4096]{2,1,0:T(8,128)(2,1)S(1)}, bf16[1,344,4096]{2,1,0:T(8,128)(2,1)}, u32[]{:S(2)}) copy-start(bf16[1,344,4096]{2,1,0:T(8,128)(2,1)} %param.13) | copy-start | bytes 8454148
  202.6 8.8 %slice-start.3 = ((s8[6291456]{0:T(1024)(128)(4,1)}), s8[4194304]{0:T(1024)(128)(4,1)S(1)}, s32[]{:S(2)}) async-start(s8[6291456]{0:T(1024)(128)(4,1)} %bitcast.57), calls=%async_computation.14 | async-start | bytes 8388608
  208.8 2.6 slice-start.4
  234.8 36.2 %reduce-scatter.3.cloned.1.call-start = ((), (), s32[]{:S(2)}) async-start(), calls=%async_computation.9 | async-start | bytes 12582912 | tf_op jit(solution)/shard_map/reduce_scatter | solution.py:105
  234.8 5.5 %copy-start.3 = (bf16[768,344]{0,1:T(8,128)(2,1)S(1)}, bf16[768,344]{0,1:T(8,128)(2,1)}, u32[]{:S(2)}) copy-start(bf16[768,344]{0,1:T(8,128)(2,1)} %get-tuple-element.7) | copy-start | bytes 1585156
  271.0 70.3 %all-to-all-start.3 = ((bf16[64,12,2048]{2,1,0:T(8,128)(2,1)}), bf16[64,12,2048]{2,1,0:T(8,128)(2,1)}, u32[]{:S(2)}, u32[]{:S(2)}) async-start(bf16[64,12,2048]{2,1,0:T(8,128)(2,1)} %reduce-scatter.3.cloned.1.call-done), calls=%async_computation.4 | async-start | bytes 8388608 | tf_op jit(solution)/shard_map/all_to_all | solution.py:116
  283.3 7.0 %copy-start.4 = (bf16[768,344]{0,1:T(8,128)(2,1)S(1)}, bf16[768,344]{0,1:T(8,128)(2,1)}, u32[]{:S(2)}) copy-start(bf16[768,344]{0,1:T(8,128)(2,1)} %get-tuple-element.7) | copy-start | bytes 1585156
  283.3 13.8 %slice-start = ((s8[12582912]{0:T(1024)(128)(4,1)}), s8[4194304]{0:T(1024)(128)(4,1)S(1)}, s32[]{:S(2)}) async-start(s8[12582912]{0:T(1024)(128)(4,1)} %bitcast.53), calls=%async_computation.11 | async-start | bytes 8388608
  283.3 13.8 %slice-start.1 = ((s8[12582912]{0:T(1024)(128)(4,1)}), s8[4194304]{0:T(1024)(128)(4,1)S(1)}, s32[]{:S(2)}) async-start(s8[12582912]{0:T(1024)(128)(4,1)} %bitcast.53), calls=%async_computation.12 | async-start | bytes 8388608
  290.2 6.9 %slice-start.2 = ((s8[12582912]{0:T(1024)(128)(4,1)}), s8[4194304]{0:T(1024)(128)(4,1)S(1)}, s32[]{:S(2)}) async-start(s8[12582912]{0:T(1024)(128)(4,1)} %bitcast.53), calls=%async_computation.13 | async-start | bytes 8388608
Sparse Core Ops, SparseCore 0:
  81.8 24.6 all-gather.2
  155.1 20.5 all-gather.4
  234.9 5.9 reduce-scatter.4
  255.9 14.9 reduce-scatter.2
where the time goes:
time: 361 us; the launch traced here: 356 us
  blocking collectives  171 us (47%)
  matrix products  54.3 us (15%)
  local copies, waits for them, and re-layouts  52.1 us (14%)
  waiting for transfers between devices  38.9 us (11%)
  other arithmetic  15.3 us (4%)
  between operations  14 us (4%)
  starting transfers between devices  11 us (3%)
    all_to_all x1, blocking collectives, per_device(): lax.all_to_all(to_slots(token_piece), 'ep', split_axis=0, concat_axis=0,...  70.4 us
    all_to_all x1, blocking collectives, per_device(): lax.all_to_all(to_slots(cot_piece), 'ep', split_axis=0, concat_axis=0, ti...  69.3 us
    all_to_all x1, waiting for transfers between devices, per_device(): lax.all_to_all(summed_rows.astype(jnp.bfloat16), 'ep', split_axis=0, conc...  38.8 us
    all_to_all x1, blocking collectives, per_device(): lax.all_to_all(share_send, 'ep', split_axis=0, concat_axis=0, tiled=True)  16.5 us
    all_to_all x1, blocking collectives, per_device(): lax.all_to_all(summed_shares.astype(jnp.bfloat16), 'ep', split_axis=0, co...  14.4 us
    convert_element_type x1, local copies, waits for them, and re-layouts, expert_pass(): rows_cot.astype(jnp.float32) * shares[:, None]  11.4 us
    all_to_all x1, starting transfers between devices, per_device(): lax.all_to_all(summed_rows.astype(jnp.bfloat16), 'ep', split_axis=0, conc...  10.8 us
    convert_element_type x1, other arithmetic, expert_pass(): (rows_cot.astype(jnp.float32) * shares[:, None]).astype(jnp.bfloat16)  10.1 us
  transfers between devices with their start and end apart: 5, of which 1 were waited for; matrix products, arithmetic and copies ran while one was open for 18% of the time, Pallas kernels for 0%

commit v1 on v0

v1 whole, which is shorter than its diff:
```python
import functools

import jax
import jax.numpy as jnp
from jax import lax
from jax.experimental import pallas as pl
from jax.experimental.pallas import tpu as pltpu
from jax.sharding import PartitionSpec as P

EXPERTS = 8
TOP = 2
CAP = 12
SIDE = 4
ROWS = 32
BUNDLE = 48
LANES = 256
BF = jnp.bfloat16
F32 = jnp.float32
MESH = pl.DeviceIdType.MESH


def dot_nt(a, b):
    return lax.dot_general(a, b, (((1,), (1,)), ((), ())), preferred_element_type=F32)


def dot_tn(a, b):
    return lax.dot_general(a, b, (((0,), (0,)), ((), ())), preferred_element_type=F32)


def dot_nn(a, b):
    return jnp.dot(a, b, preferred_element_type=F32)


def kernel(
    nc, hid,
    src, info, gate, up, down,
    out_tok, out_rg, out_gate, out_up, out_down,
    tz, iz, xc, ob, place, place_t, share,
    stg, stu, wd, wc, pre, hg, gsus, hid_t,
    part, tps, tpr, s_f, xa_f, xb_f, yr_f, zs_f, zr_f,
    part_r, tpr_r, s_r, xa_r, xb_r, yr_r, zs_r, zr_r,
    w_sem, z_send, z_recv, y_send, y_recv, x_send, x_recv, d_send, d_recv,
    e_send, e_recv, a_send, a_recv, b_send, b_recv, v_send, v_recv, q_send, q_recv,
    o_sem,
):
    ep = lax.axis_index("ep")
    core = lax.axis_index("tp")
    z, y, x = ep // 16, (ep // 4) % 4, ep % 4
    pair = y // 2
    low = 256
    rest = hid - low

    def chip(zz, yy, xx):
        return (zz * 16 + yy * 4 + xx, core)

    right = chip(z, y, (x + 1) % 4)
    left = chip(z, y, (x + 3) % 4)
    other_core = (ep, 1 - core)
    partner_y = 2 * pair + (1 - y % 2)
    cross_y = 3 - y
    cross2_y = 2 * (1 - pair) + y % 2
    y_peers = [partner_y, cross_y, cross2_y]
    z_peers = [(z + 1) % 4, (z + 3) % 4, (z + 2) % 4]

    barrier = pltpu.get_barrier_semaphore()
    for zz in z_peers:
        pl.semaphore_signal(barrier, inc=1, device_id=chip(zz, y, x), device_id_type=MESH)
    for yy in y_peers:
        pl.semaphore_signal(barrier, inc=1, device_id=chip(z, yy, x), device_id_type=MESH)
    for dev in (right, left, other_core):
        pl.semaphore_signal(barrier, inc=1, device_id=dev, device_id_type=MESH)

    w_copies = [
        pltpu.make_async_copy(gate.at[0], stg, w_sem.at[0]),
        pltpu.make_async_copy(up.at[0], stu, w_sem.at[1]),
    ]
    for k in range(2 * nc):
        w_copies.append(
            pltpu.make_async_copy(
                down.at[0, :, pl.ds(k * LANES, LANES)], wd.at[k], w_sem.at[2 + k]
            )
        )
    for cp in w_copies:
        cp.start()

    pl.semaphore_wait(barrier, 9)

    def remote(a, b, ss, rs, dev):
        return pltpu.make_async_remote_copy(
            src_ref=a, dst_ref=b, send_sem=ss, recv_sem=rs, device_id=dev, device_id_type=MESH
        )

    def z_copy(c, i):
        return remote(
            src.at[c], tz.at[c, z], z_send.at[c, i], z_recv.at[c, i], chip(z_peers[i], y, x)
        )

    def zi_copy(i):
        return remote(
            info, iz.at[i + 1], z_send.at[nc, i], z_recv.at[nc, i], chip(z_peers[i], y, x)
        )

    for i in range(3):
        zi_copy(i).start()

    def start_z(c, carry):
        for i in range(3):
            z_copy(c, i).start()
        return carry

    lax.fori_loop(0, nc, start_z, 0)

    iz[0] = info[...]
    pre[...] = jnp.zeros_like(pre)
    hg[...] = jnp.zeros_like(hg)
    for i in range(3):
        zi_copy(i).wait_recv()

    slot_number = lax.broadcasted_iota(jnp.int32, (BUNDLE, 128), 0).astype(F32) + 1.0

    def info_row(kind, expert):
        total = iz[0, kind, pl.ds(expert, 1), :]
        for i in range(1, 4):
            total = total + iz[i, kind, pl.ds(expert, 1), :]
        return total

    spare = jnp.zeros((128 - 2 * BUNDLE, 128), F32)
    first, second = [], []
    for side, expert in ((0, 2 * z + pair), (1, 2 * z + 1 - pair)):
        first.append(jnp.where(slot_number == info_row(0, expert), 1.0, 0.0))
        second.append(jnp.where(slot_number == info_row(1, expert), 1.0, 0.0))
        share[side * BUNDLE:(side + 1) * BUNDLE, :] = jnp.broadcast_to(
            jnp.sum((first[side] + second[side]) * info_row(2, expert), axis=1, keepdims=True),
            (BUNDLE, 128),
        )
    first = jnp.concatenate(first + [spare], axis=0)
    second = jnp.concatenate(second + [spare], axis=0)
    place[...] = (first + second).astype(BF)
    place_t[0] = (first + second).T.astype(BF)
    place_t[1] = first.T.astype(BF)
    place_t[2] = second.T.astype(BF)

    def y_copy(c, i):
        k = core * nc + c
        at = pl.ds(x * 192 + y * BUNDLE, BUNDLE)
        from_ref = xc.at[k, :, at, :] if i == 0 else ob.at[c]
        return remote(
            from_ref, xc.at[k, :, at, :], y_send.at[c, i], y_recv.at[c, i],
            chip(z, y_peers[i], x),
        )

    def y_arrival(c, i):
        k = core * nc + c
        at = pl.ds(x * 192 + y_peers[i] * BUNDLE, BUNDLE)
        return remote(
            ob.at[c], xc.at[k, :, at, :], y_send.at[c, i], y_recv.at[c, i],
            chip(z, y_peers[i], x),
        )

    def x_copy(c, i):
        k = core * nc + c
        if i < 2:
            at = pl.ds(x * 192, 192)
        elif i == 2:
            at = pl.ds(((x + 3) % 4) * 192, 96)
        else:
            at = pl.ds(((x + 1) % 4) * 192 + 96, 96)
        return remote(
            xc.at[k, :, at, :], xc.at[k, :, at, :], x_send.at[c, i], x_recv.at[c, i],
            right if i % 2 == 0 else left,
        )

    def x_arrival(c, i):
        k = core * nc + c
        if i == 0:
            at = pl.ds(((x + 3) % 4) * 192, 192)
        elif i == 1:
            at = pl.ds(((x + 1) % 4) * 192, 192)
        elif i == 2:
            at = pl.ds(((x + 2) % 4) * 192, 96)
        else:
            at = pl.ds(((x + 2) % 4) * 192 + 96, 96)
        return remote(
            xc.at[k, :, at, :], xc.at[k, :, at, :], x_send.at[c, i], x_recv.at[c, i],
            right if i % 2 == 0 else left,
        )

    def d_copy(c, k):
        return remote(xc.at[k], xc.at[k], d_send.at[c], d_recv.at[c], other_core)

    def compact(c):
        for i in range(3):
            z_copy(c, i).wait_recv()
        k = core * nc + c
        at = pl.ds(pl.multiple_of(x * 192 + y * BUNDLE, BUNDLE), BUNDLE)
        for tensor in range(2):
            rows = dot_nn(place[:2 * BUNDLE], tz[c, :, tensor].reshape(SIDE * ROWS, LANES))
            if tensor == 1:
                rows = rows * share[:, 0:1]
            rows = rows.astype(BF)
            xc[k, tensor, at, :] = rows[:BUNDLE]
            ob[c, tensor] = rows[BUNDLE:]
        for i in range(3):
            y_copy(c, i).start()

    def products(k):
        for m in range(3):
            rows = pl.ds(m * 256, 256)
            pre[rows, :] += dot_nn(xc[k, 0, rows, :], wc[k])
            hg[rows, :hid] += dot_nt(xc[k, 1, rows, :], wd[k])

    def assemble(k, carry):
        rows = pl.ds(pl.multiple_of(k * LANES, LANES), LANES)
        wc[k, :, 512:768] = jnp.zeros((LANES, 256), BF)
        wc[k, :, 0:256] = stg[rows, 0:256]
        wc[k, :, 256:512] = stu[rows, 0:256]
        wc[k, :, 512:512 + rest] = stg[rows, 256:hid]
        wc[k, :, 640:640 + rest] = stu[rows, 256:hid]
        return carry

    def dispatch(t, carry):
        @pl.when(t < nc)
        def _():
            compact(t)

        @pl.when((t >= 1) & (t < nc + 1))
        def _():
            for i in range(3):
                y_arrival(t - 1, i).wait_recv()
            for i in range(2):
                x_copy(t - 1, i).start()

        @pl.when(t == 1)
        def _():
            for cp in w_copies:
                cp.wait()
            lax.fori_loop(0, 2 * nc, assemble, 0)

        @pl.when((t >= 2) & (t < nc + 2))
        def _():
            for i in range(2):
                x_arrival(t - 2, i).wait_recv()
            for i in range(2, 4):
                x_copy(t - 2, i).start()

        @pl.when((t >= 3) & (t < nc + 3))
        def _():
            for i in range(2, 4):
                x_arrival(t - 3, i).wait_recv()
            d_copy(t - 3, core * nc + t - 3).start()
            products(core * nc + t - 3)

        @pl.when(t >= 4)
        def _():
            d_copy(t - 4, (1 - core) * nc + t - 4).wait_recv()
            products((1 - core) * nc + t - 4)

        return carry

    def own_rows(c, carry):
        tz[c, z] = src[c]
        return carry

    lax.fori_loop(0, nc, own_rows, 0)
    lax.fori_loop(0, nc + 4, dispatch, 0)

    def gates(m, carry):
        rows = pl.ds(pl.multiple_of(m * 128, 128), 128)
        value = jnp.zeros((128, 1), F32)
        for g_at, u_at, h_at, n in ((0, 256, 0, 256), (512, 640, 256, 128)):
            g = pre[rows, g_at:g_at + n]
            u = pre[rows, u_at:u_at + n]
            h = hg[rows, h_at:h_at + n]
            s = jax.nn.sigmoid(g)
            active = g * s
            hidden = (active * u).astype(BF)
            gsus[rows, g_at:g_at + n] = (h * u * (s * (1.0 + g * (1.0 - s)))).astype(BF)
            gsus[rows, u_at:u_at + n] = (h * active).astype(BF)
            hidden = hidden.astype(F32)
            value = value + jnp.sum(hidden * h, axis=1, keepdims=True)
            hid_t[h_at:h_at + n, rows] = hidden.T.astype(BF)
        part_r[rows, :] = jnp.broadcast_to(value, (128, 128)).astype(BF)
        return carry

    lax.fori_loop(0, 6, gates, 0)

    def e_copy(n, feature, c):
        if feature:
            return remote(tps.at[c], tpr.at[c], e_send.at[n], e_recv.at[n], other_core)
        return remote(part_r, tpr_r, e_send.at[n], e_recv.at[n], other_core)

    def pick(feature, c, f_ref, r_ref):
        return f_ref.at[c] if feature else r_ref

    def a_copy(n, feature, c, i):
        s, xa = pick(feature, c, s_f, s_r), pick(feature, c, xa_f, xa_r)
        at = pl.ds(((x + 2) % 4) * 192 + 96 * i, 96)
        return remote(
            s.at[at], xa.at[i], a_send.at[n, i], a_recv.at[n, i], right if i == 0 else left
        )

    def b_copy(n, feature, c, i):
        s, xb = pick(feature, c, s_f, s_r), pick(feature, c, xb_f, xb_r)
        at = pl.ds(((x + 1 + 2 * i) % 4) * 192, 192)
        return remote(
            s.at[at], xb.at[i], b_send.at[n, i], b_recv.at[n, i], right if i == 0 else left
        )

    def v_copy(n, feature, c, i):
        s, yr = pick(feature, c, s_f, s_r), pick(feature, c, yr_f, yr_r)
        at = pl.ds(x * 192 + y_peers[i] * BUNDLE, BUNDLE)
        return remote(
            s.at[at], yr.at[i], v_send.at[n, i], v_recv.at[n, i], chip(z, y_peers[i], x)
        )

    def q_copy(n, feature, c, i):
        zs, zr = pick(feature, c, zs_f, zs_r), pick(feature, c, zr_f, zr_r)
        return remote(
            zs.at[z_peers[i]], zr.at[i], q_send.at[n, i], q_recv.at[n, i], chip(z_peers[i], y, x)
        )

    def stage_core(n, feature, c):
        if not feature:
            e_copy(n, False, c).start()
            return
        k = (1 - core) * nc + c
        for m in range(3):
            rows = pl.ds(m * 256, 256)
            tps[c, rows, :] = dot_nt(gsus[rows, :], wc[k]).astype(BF)
        e_copy(n, True, c).start()
        k = core * nc + c
        for m in range(3):
            rows = pl.ds(m * 256, 256)
            part[c % 2, rows, :] = dot_nt(gsus[rows, :], wc[k])

    def stage_a(n, feature, c):
        e_copy(n, feature, c).wait_recv()
        s = pick(feature, c, s_f, s_r)
        mine = part.at[c % 2] if feature else part_r
        theirs = pick(feature, c, tpr, tpr_r)
        for m in range(3):
            rows = pl.ds(m * 256, 256)
            s[rows, :] = (mine[rows, :].astype(F32) + theirs[rows, :].astype(F32)).astype(BF)
        for i in range(2):
            a_copy(n, feature, c, i).start()

    def stage_b(n, feature, c):
        s, xa = pick(feature, c, s_f, s_r), pick(feature, c, xa_f, xa_r)
        for i in range(2):
            a_copy(n, feature, c, i).wait_recv()
            at = pl.ds(pl.multiple_of(((x + 1 + 2 * i) % 4) * 192 + 96 * i, 96), 96)
            s[at, :] = (s[at, :].astype(F32) + xa[i].astype(F32)).astype(BF)
        for i in range(2):
            b_copy(n, feature, c, i).start()

    def stage_v(n, feature, c):
        s, xb = pick(feature, c, s_f, s_r), pick(feature, c, xb_f, xb_r)
        for i in range(2):
            b_copy(n, feature, c, i).wait_recv()
        at = pl.ds(pl.multiple_of(x * 192, 192), 192)
        s[at, :] = (s[at, :].astype(F32) + xb[0].astype(F32) + xb[1].astype(F32)).astype(BF)
        for i in range(3):
            v_copy(n, feature, c, i).start()

    def stage_q(n, feature, c):
        s, yr = pick(feature, c, s_f, s_r), pick(feature, c, yr_f, yr_r)
        zs = pick(feature, c, zs_f, zs_r)
        for i in range(3):
            v_copy(n, feature, c, i).wait_recv()
        at = pl.ds(pl.multiple_of(x * 192 + y * BUNDLE, BUNDLE), BUNDLE)
        mine = (s[at, :].astype(F32) + yr[0].astype(F32)).astype(BF)
        theirs = (yr[1].astype(F32) + yr[2].astype(F32)).astype(BF)
        slots = jnp.concatenate(
            [mine, theirs, jnp.zeros((128 - 2 * BUNDLE, mine.shape[1]), BF)], axis=0
        )
        if feature:
            rows = dot_nn(place_t[0], slots)
        else:
            lane = lax.broadcasted_iota(jnp.int32, (SIDE * ROWS, 128), 1)
            rows = jnp.where(
                lane == 0,
                dot_nn(place_t[1], slots),
                dot_nn(place_t[2], slots),
            )
        zs[...] = rows.astype(BF).reshape(zs.shape)
        for i in range(3):
            q_copy(n, feature, c, i).start()

    def stage_out(n, feature, c):
        zs, zr = pick(feature, c, zs_f, zs_r), pick(feature, c, zr_f, zr_r)
        for i in range(3):
            q_copy(n, feature, c, i).wait_recv()
        total = zs[z].astype(F32)
        for i in range(3):
            total = total + zr[i].astype(F32)
        if feature:
            out_tok[:, pl.ds(pl.multiple_of(c * LANES, LANES), LANES)] = total[:24].astype(BF)
        else:
            out_rg[...] = total

    def out_copies(k):
        rows = pl.ds(pl.multiple_of(k * LANES, LANES), LANES)
        return (
            pltpu.make_async_copy(stg.at[rows], out_gate.at[0, rows], o_sem.at[k, 0]),
            pltpu.make_async_copy(stu.at[rows], out_up.at[0, rows], o_sem.at[k, 1]),
            pltpu.make_async_copy(wd.at[k], out_down.at[0, :, rows], o_sem.at[k, 2]),
        )

    def weight_grads(k):
        rows = pl.ds(pl.multiple_of(k * LANES, LANES), LANES)
        both = dot_tn(xc[k, 0], gsus[...]).astype(BF)
        stg[rows, 0:256] = both[:, 0:256]
        stu[rows, 0:256] = both[:, 256:512]
        stg[rows, 256:hid] = both[:, 512:512 + rest]
        stu[rows, 256:hid] = both[:, 640:640 + rest]
        wd[k] = dot_nn(hid_t[:hid], xc[k, 1]).astype(BF)
        for cp in out_copies(k):
            cp.start()

    stages = (stage_core, stage_a, stage_b, stage_v, stage_q, stage_out)

    def give_back(t, carry):
        for depth, stage in enumerate(stages):
            n = t - depth

            @pl.when(n == 0)
            def _():
                stage(0, False, 0)

            @pl.when((n >= 1) & (n <= nc))
            def _():
                stage(n, True, n - 1)

        @pl.when(t < nc)
        def _():
            weight_grads(2 * t)
            weight_grads(2 * t + 1)

        return carry

    lax.fori_loop(0, nc + 1 + len(stages) - 1, give_back, 0)

    for i in range(3):
        zi_copy(i).wait_send()

    def drain_dispatch(c, carry):
        for i in range(3):
            z_copy(c, i).wait_send()
            y_copy(c, i).wait_send()
        for i in range(4):
            x_copy(c, i).wait_send()
        d_copy(c, core * nc + c).wait_send()
        return carry

    lax.fori_loop(0, nc, drain_dispatch, 0)

    def drain_return(n, feature, c):
        e_copy(n, feature, c).wait_send()
        for i in range(2):
            a_copy(n, feature, c, i).wait_send()
            b_copy(n, feature, c, i).wait_send()
        for i in range(3):
            v_copy(n, feature, c, i).wait_send()
            q_copy(n, feature, c, i).wait_send()

    drain_return(0, False, 0)

    def drain_features(n, carry):
        drain_return(n, True, n - 1)
        return carry

    lax.fori_loop(1, nc + 1, drain_features, 0)

    def drain_outputs(k, carry):
        for cp in out_copies(k):
            cp.wait()
        return carry

    lax.fori_loop(0, 2 * nc, drain_outputs, 0)


def per_device(tokens, cotangent, routes, route_weights, gate_weight, up_weight, down_weight):
    ep = lax.axis_index("ep")
    core = lax.axis_index("tp")
    z = ep // 16
    rows, width = tokens.shape
    half = width // lax.axis_size("tp")
    nc = half // LANES
    hid = gate_weight.shape[2]

    def halves(a):
        piece = lax.dynamic_slice_in_dim(a, core * half, half, 1)
        piece = jnp.pad(piece, ((0, ROWS - rows), (0, 0)))
        return piece.reshape(ROWS, nc, LANES).transpose(1, 0, 2)

    src = jnp.stack([halves(tokens), halves(cotangent)], axis=1)

    hot = routes[:, :, None] == jnp.arange(EXPERTS, dtype=jnp.int32)[None, None, :]
    hit = jnp.any(hot, axis=1)
    earlier = jnp.arange(rows)[:, None] > jnp.arange(rows)[None, :]
    position = jnp.sum((earlier[:, :, None] & hit[None, :, :]).astype(jnp.int32), axis=1)
    code = (position + z * CAP + 1).astype(F32)
    kinds = jnp.stack(
        [
            jnp.where(hot[:, 0], code, 0.0),
            jnp.where(hot[:, 1], code, 0.0),
            jnp.sum(jnp.where(hot, route_weights[:, :, None], 0.0), axis=1),
        ]
    )
    info = jnp.pad(kinds.transpose(0, 2, 1), ((0, 0), (0, 0), (0, ROWS - rows)))
    column = jnp.arange(SIDE, dtype=jnp.int32) == z
    info = jnp.where(column[None, None, :, None], info[:, :, None, :], 0.0)
    info = info.reshape(3, EXPERTS, SIDE * ROWS)

    vmem, anywhere = pltpu.VMEM, pl.ANY
    slots = 16 * BUNDLE

    def chunk_buffers(lead, lanes):
        return [
            vmem((*lead, slots, lanes), BF),
            vmem((*lead, 2, 96, lanes), BF),
            vmem((*lead, 2, 192, lanes), BF),
            vmem((*lead, 3, BUNDLE, lanes), BF),
            vmem((*lead, SIDE, ROWS, lanes), BF),
            vmem((*lead, 3, ROWS, lanes), BF),
        ]

    dma = pltpu.SemaphoreType.DMA
    token_grad, shares, gate_grad, up_grad, down_grad = pl.pallas_call(
        functools.partial(kernel, nc, hid),
        out_shape=(
            jax.ShapeDtypeStruct((rows, half), BF),
            jax.ShapeDtypeStruct((ROWS, 128), F32),
            jax.ShapeDtypeStruct(gate_weight.shape, BF),
            jax.ShapeDtypeStruct(up_weight.shape, BF),
            jax.ShapeDtypeStruct(down_weight.shape, BF),
        ),
        in_specs=[
            pl.BlockSpec(memory_space=vmem),
            pl.BlockSpec(memory_space=vmem),
            pl.BlockSpec(memory_space=anywhere),
            pl.BlockSpec(memory_space=anywhere),
            pl.BlockSpec(memory_space=anywhere),
        ],
        out_specs=(
            pl.BlockSpec(memory_space=vmem),
            pl.BlockSpec(memory_space=vmem),
            pl.BlockSpec(memory_space=anywhere),
            pl.BlockSpec(memory_space=anywhere),
            pl.BlockSpec(memory_space=anywhere),
        ),
        scratch_shapes=[
            vmem((nc, SIDE, 2, ROWS, LANES), BF),
            vmem((SIDE, 3, EXPERTS, 128), F32),
            vmem((2 * nc, 2, slots, LANES), BF),
            vmem((nc, 2, BUNDLE, LANES), BF),
            vmem((128, 128), BF),
            vmem((3, 128, 128), BF),
            vmem((2 * BUNDLE, 128), F32),
            vmem((width, hid), BF),
            vmem((width, hid), BF),
            vmem((2 * nc, hid, LANES), BF),
            vmem((2 * nc, LANES, 768), BF),
            vmem((slots, 768), F32),
            vmem((slots, 384), F32),
            vmem((slots, 768), BF),
            vmem((384, slots), BF),
            vmem((2, slots, LANES), F32),
            vmem((nc, slots, LANES), BF),
            vmem((nc, slots, LANES), BF),
            *chunk_buffers((nc,), LANES),
            vmem((slots, 128), BF),
            vmem((slots, 128), BF),
            *chunk_buffers((), 128),
            dma((2 + 2 * nc,)),
            dma((nc + 1, 3)), dma((nc + 1, 3)),
            dma((nc, 3)), dma((nc, 3)),
            dma((nc, 4)), dma((nc, 4)),
            dma((nc,)), dma((nc,)),
            dma((nc + 1,)), dma((nc + 1,)),
            dma((nc + 1, 2)), dma((nc + 1, 2)),
            dma((nc + 1, 2)), dma((nc + 1, 2)),
            dma((nc + 1, 3)), dma((nc + 1, 3)),
            dma((nc + 1, 3)), dma((nc + 1, 3)),
            dma((2 * nc, 3)),
        ],
        compiler_params=pltpu.CompilerParams(
            collective_id=0, has_side_effects=True, vmem_limit_bytes=63 * 1024 * 1024
        ),
    )(src, info, gate_weight, up_weight, down_weight)
    route_grad = shares[:rows, :TOP] / route_weights
    return token_grad, route_grad, gate_grad, up_grad, down_grad


def solution(mesh):
    return jax.shard_map(
        per_device,
        mesh=mesh,
        in_specs=(
            P("ep", None),
            P("ep", None),
            P("ep", None),
            P("ep", None),
            P("ep", None, "tp"),
            P("ep", None, "tp"),
            P("ep", "tp", None),
        ),
        out_specs=(
            P("ep", "tp"),
            P("ep", None),
            P("ep", None, "tp"),
            P("ep", None, "tp"),
            P("ep", "tp", None),
        ),
        check_vma=False,
    )
```

time: 361 us -> 152 us (0.42); the launches traced: 356 us -> 152 us
  blocking collectives: 171 us -> 0 us
  Pallas kernels: 0 us -> 126 us
  matrix products: 54.3 us -> 0 us
  waiting for transfers between devices: 38.9 us -> 0 us
  local copies, waits for them, and re-layouts: 52.1 us -> 21.6 us
  between operations: 14 us -> 0.76 us
  other arithmetic: 15.3 us -> 3.4 us
  starting transfers between devices: 11 us -> 0 us
    all_to_all x4 -> x0, blocking collectives: 171 us -> none  [the longest x1 70.4 us: per_device(): lax.all_to_all(to_slots(token_piece), 'ep', split_axis=0, concat_axis=0,...]
    pallas_call x0 -> x1, Pallas kernels: none -> 126 us  [per_device(): pl.pallas_call(functools.partial(kernel, nc, hid), out_shape=(jax.ShapeDt...]
    dot_general x14 -> x0, matrix products: 54.3 us -> none  [the longest x1 7.49 us: expert_pass(): expert_out = jnp.dot(hidden, down_mat, preferred_element_type=jnp.float32)]
    all_to_all x1 -> x0, waiting for transfers between devices: 38.8 us -> none  [per_device(): lax.all_to_all(summed_rows.astype(jnp.bfloat16), 'ep', split_axis=0, conc...]
    convert_element_type x5 -> x0, local copies, waits for them, and re-layouts: 31.2 us -> none  [the longest x1 11.4 us: expert_pass(): rows_cot.astype(jnp.float32) * shares[:, None]]
    unnamed x24 -> x19, local copies, waits for them, and re-layouts: 1.69 us -> 20.1 us
    reshape x8 -> x2, local copies, waits for them, and re-layouts: 12.6 us -> 0.02 us  [halves(): return piece.reshape(ROWS, nc, LANES).transpose(1, 0, 2)]
    all_to_all x1 -> x0, starting transfers between devices: 10.8 us -> none  [per_device(): lax.all_to_all(summed_rows.astype(jnp.bfloat16), 'ep', split_axis=0, conc...]
  transfers between devices with their start and end apart: 5 -> 0, of which waited for: 1 -> 0; matrix products, arithmetic and copies ran while one was open for 18% -> 0% of each run, Pallas kernels for 0% -> 0%
where the time goes in v1:
time: 152 us
  Pallas kernels  126 us (83%)
  local copies, waits for them, and re-layouts  21.6 us (14%)
  other arithmetic  3.4 us (2%)
    pallas_call x1, Pallas kernels, per_device(): pl.pallas_call(functools.partial(kernel, nc, hid), out_shape=(jax.ShapeDt...  126 us
    unnamed x19, local copies, waits for them, and re-layouts  20.1 us

profile of v1, /device:TPU:0, one launch (start us, length us, event | category | flops | bytes accessed | tf_op | source)
XLA Modules:
  0.0 151.7 jit_solution(14920328027421277267)
XLA Ops:
  0.6 0.8 fusion
  1.4 0.1 copy.68
  1.5 0.5 convert_reduce_fusion
  2.0 0.1 copy.59
  2.1 0.1 copy.60
  2.1 0.8 select_reduce_fusion
  2.9 0.1 copy.61
  3.0 0.1 broadcast_in_dim.59
  3.1 0.1 broadcast_in_dim.52
  3.2 0.1 broadcast_in_dim.53
  3.3 0.6 broadcast_select_fusion.info
  3.9 1.0 constant_dynamic-slice_fusion
  4.9 0.7 pad_maximum_fusion.src
  5.7 4.7 %copy.62.gate = bf16[1,4096,344]{2,1,0:T(8,128)(2,1)} copy(bf16[1,4096,344]{1,2,0:T(8,128)(2,1)} %param.11) | data formatting | bytes 5636096 | tf_op args[4]
  10.4 0.0 copy-done.1
  10.4 2.8 %copy.63.up = bf16[1,4096,344]{2,1,0:T(8,128)(2,1)} copy(bf16[1,4096,344]{1,2,0:T(8,128)(2,1)S(1)} %copy-done.1) | data formatting | bytes 5636096 | tf_op args[5]
  13.2 125.9 %shard_map.110 = (bf16[24,2048]{1,0:T(8,128)(2,1)}, f32[32,128]{1,0:T(8,128)}, bf16[1,4096,344]{2,1,0:T(8,128)(2,1)}, bf16[1,4096,344]{2,1,0:T(8,128)(2,1)}, bf16[1,344,4096]{2,1,0:T(8,128)(2,1)}) custom-call(bf16[8,2,32,256]{3,2,1,0:T(8,128)(2,1)} %pad_maximum_fusion.src, f32[3,8,128]{2,1,0:T(8,128)} %broadcast_select_fusion.info, ...), custom_call_target="tpu_custom_call" | custom-call | tf_op jit(solution)/shard_map/pallas_call | solution.py:529
  139.1 0.0 copy-start
  139.1 4.7 %copy.66 = bf16[1,4096,344]{1,2,0:T(8,128)(2,1)} copy(bf16[1,4096,344]{2,1,0:T(8,128)(2,1)} %get-tuple-element.42) | data formatting | bytes 5636096
  143.8 2.8 %copy.67 = bf16[1,4096,344]{1,2,0:T(8,128)(2,1)} copy(bf16[1,4096,344]{2,1,0:T(8,128)(2,1)S(1)} %copy-done) | data formatting | bytes 5636096
  146.6 0.1 copy.64
  146.7 0.6 copy.65
  147.4 0.6 copy.77
  148.0 3.7 %copy.78 = bf16[1,344,4096]{2,1,0:T(8,128)(2,1)} copy(bf16[1,344,4096]{2,1,0:T(8,128)(2,1)} %get-tuple-element.60) | data formatting | bytes 5636096
  (19 shorter events, 0.1 us)
Async XLA Ops:
  5.7 4.7 %copy-start.1 = (bf16[1,4096,344]{1,2,0:T(8,128)(2,1)S(1)}, bf16[1,4096,344]{1,2,0:T(8,128)(2,1)}, u32[]{:S(2)}) copy-start(bf16[1,4096,344]{1,2,0:T(8,128)(2,1)} %param.12) | copy-start | bytes 8454148
  139.1 4.7 %copy-start = (bf16[1,4096,344]{2,1,0:T(8,128)(2,1)S(1)}, bf16[1,4096,344]{2,1,0:T(8,128)(2,1)}, u32[]{:S(2)}) copy-start(bf16[1,4096,344]{2,1,0:T(8,128)(2,1)} %get-tuple-element.43) | copy-start | bytes 8454148
  143.8 2.8 %copy-start.4 = (f32[24,2]{0,1:T(2,128)S(1)}, f32[24,2]{0,1:T(2,128)}, u32[]{:S(2)}) copy-start(f32[24,2]{0,1:T(2,128)} %param.10) | copy-start | bytes 580
  143.8 2.9 %copy-start.3 = (f32[32,128]{1,0:T(8,128)S(1)}, f32[32,128]{1,0:T(8,128)}, u32[]{:S(2)}) copy-start(f32[32,128]{1,0:T(8,128)} %get-tuple-element.11) | copy-start | bytes 49156
  143.8 3.5 %copy-start.2 = (bf16[24,2048]{1,0:T(8,128)(2,1)S(1)}, bf16[24,2048]{1,0:T(8,128)(2,1)}, u32[]{:S(2)}) copy-start(bf16[24,2048]{1,0:T(8,128)(2,1)} %get-tuple-element.56) | copy-start | bytes 294916

commit v2 on v1

--- a/solution.py
+++ b/solution.py
@@ -14,6 +14,7 @@
 ROWS = 32
 BUNDLE = 48
 LANES = 256
+SIDE_HID = 384
 BF = jnp.bfloat16
 F32 = jnp.float32
 MESH = pl.DeviceIdType.MESH
@@ -36,7 +37,7 @@
     src, info, gate, up, down,
     out_tok, out_rg, out_gate, out_up, out_down,
     tz, iz, xc, ob, place, place_t, share,
-    stg, stu, wd, wc, pre, hg, gsus, hid_t,
+    wd, wc, pre, hg, gsus, gsus_t, hid_t,
     part, tps, tpr, s_f, xa_f, xb_f, yr_f, zs_f, zr_f,
     part_r, tpr_r, s_r, xa_r, xb_r, yr_r, zs_r, zr_r,
     w_sem, z_send, z_recv, y_send, y_recv, x_send, x_recv, d_send, d_recv,
@@ -47,8 +48,6 @@
     core = lax.axis_index("tp")
     z, y, x = ep // 16, (ep // 4) % 4, ep % 4
     pair = y // 2
-    low = 256
-    rest = hid - low
 
     def chip(zz, yy, xx):
         return (zz * 16 + yy * 4 + xx, core)
@@ -70,16 +69,14 @@
     for dev in (right, left, other_core):
         pl.semaphore_signal(barrier, inc=1, device_id=dev, device_id_type=MESH)
 
-    w_copies = [
-        pltpu.make_async_copy(gate.at[0], stg, w_sem.at[0]),
-        pltpu.make_async_copy(up.at[0], stu, w_sem.at[1]),
-    ]
+    w_copies = []
     for k in range(2 * nc):
-        w_copies.append(
-            pltpu.make_async_copy(
-                down.at[0, :, pl.ds(k * LANES, LANES)], wd.at[k], w_sem.at[2 + k]
-            )
-        )
+        at = pl.ds(k * LANES, LANES)
+        w_copies += [
+            pltpu.make_async_copy(gate.at[0, :, at], wc.at[k, pl.ds(0, hid)], w_sem.at[k, 0]),
+            pltpu.make_async_copy(up.at[0, :, at], wc.at[k, pl.ds(SIDE_HID, hid)], w_sem.at[k, 1]),
+            pltpu.make_async_copy(down.at[0, :, at], wd.at[k], w_sem.at[k, 2]),
+        ]
     for cp in w_copies:
         cp.start()
 
@@ -206,17 +203,15 @@
     def products(k):
         for m in range(3):
             rows = pl.ds(m * 256, 256)
-            pre[rows, :] += dot_nn(xc[k, 0, rows, :], wc[k])
+            pre[rows, :] += dot_nt(xc[k, 0, rows, :], wc[k])
             hg[rows, :hid] += dot_nt(xc[k, 1, rows, :], wd[k])
 
-    def assemble(k, carry):
-        rows = pl.ds(pl.multiple_of(k * LANES, LANES), LANES)
-        wc[k, :, 512:768] = jnp.zeros((LANES, 256), BF)
-        wc[k, :, 0:256] = stg[rows, 0:256]
-        wc[k, :, 256:512] = stu[rows, 0:256]
-        wc[k, :, 512:512 + rest] = stg[rows, 256:hid]
-        wc[k, :, 640:640 + rest] = stu[rows, 256:hid]
-        return carry
+    def blank(k, carry):
+        for at in (hid, SIDE_HID + hid):
+            wc[k, at:at + SIDE_HID - hid, :] = jnp.zeros((SIDE_HID - hid, LANES), BF)
+        return carry
+
+    lax.fori_loop(0, 2 * nc, blank, 0)
 
     def dispatch(t, carry):
         @pl.when(t < nc)
@@ -234,7 +229,6 @@
         def _():
             for cp in w_copies:
                 cp.wait()
-            lax.fori_loop(0, 2 * nc, assemble, 0)
 
         @pl.when((t >= 2) & (t < nc + 2))
         def _():
@@ -267,18 +261,21 @@
     def gates(m, carry):
         rows = pl.ds(pl.multiple_of(m * 128, 128), 128)
         value = jnp.zeros((128, 1), F32)
-        for g_at, u_at, h_at, n in ((0, 256, 0, 256), (512, 640, 256, 128)):
-            g = pre[rows, g_at:g_at + n]
-            u = pre[rows, u_at:u_at + n]
-            h = hg[rows, h_at:h_at + n]
+        for at in range(0, SIDE_HID, 128):
+            g = pre[rows, at:at + 128]
+            u = pre[rows, SIDE_HID + at:SIDE_HID + at + 128]
+            h = hg[rows, at:at + 128]
             s = jax.nn.sigmoid(g)
             active = g * s
-            hidden = (active * u).astype(BF)
-            gsus[rows, g_at:g_at + n] = (h * u * (s * (1.0 + g * (1.0 - s)))).astype(BF)
-            gsus[rows, u_at:u_at + n] = (h * active).astype(BF)
-            hidden = hidden.astype(F32)
+            hidden = (active * u).astype(BF).astype(F32)
+            g_side = h * u * (s * (1.0 + g * (1.0 - s)))
+            u_side = h * active
             value = value + jnp.sum(hidden * h, axis=1, keepdims=True)
-            hid_t[h_at:h_at + n, rows] = hidden.T.astype(BF)
+            gsus[rows, at:at + 128] = g_side.astype(BF)
+            gsus[rows, SIDE_HID + at:SIDE_HID + at + 128] = u_side.astype(BF)
+            hid_t[at:at + 128, rows] = hidden.T.astype(BF)
+            gsus_t[at:at + 128, rows] = g_side.T.astype(BF)
+            gsus_t[SIDE_HID + at:SIDE_HID + at + 128, rows] = u_side.T.astype(BF)
         part_r[rows, :] = jnp.broadcast_to(value, (128, 128)).astype(BF)
         return carry
 
@@ -326,12 +323,12 @@
         k = (1 - core) * nc + c
         for m in range(3):
             rows = pl.ds(m * 256, 256)
-            tps[c, rows, :] = dot_nt(gsus[rows, :], wc[k]).astype(BF)
+            tps[c, rows, :] = dot_nn(gsus[rows, :], wc[k]).astype(BF)
         e_copy(n, True, c).start()
         k = core * nc + c
         for m in range(3):
             rows = pl.ds(m * 256, 256)
-            part[c % 2, rows, :] = dot_nt(gsus[rows, :], wc[k])
+            part[c % 2, rows, :] = dot_nn(gsus[rows, :], wc[k])
 
     def stage_a(n, feature, c):
         e_copy(n, feature, c).wait_recv()
@@ -399,20 +396,17 @@
             out_rg[...] = total
 
     def out_copies(k):
-        rows = pl.ds(pl.multiple_of(k * LANES, LANES), LANES)
+        at = pl.ds(pl.multiple_of(k * LANES, LANES), LANES)
         return (
-            pltpu.make_async_copy(stg.at[rows], out_gate.at[0, rows], o_sem.at[k, 0]),
-            pltpu.make_async_copy(stu.at[rows], out_up.at[0, rows], o_sem.at[k, 1]),
-            pltpu.make_async_copy(wd.at[k], out_down.at[0, :, rows], o_sem.at[k, 2]),
+            pltpu.make_async_copy(wc.at[k, pl.ds(0, hid)], out_gate.at[0, :, at], o_sem.at[k, 0]),
+            pltpu.make_async_copy(wc.at[k, pl.ds(SIDE_HID, hid)], out_up.at[0, :, at], o_sem.at[k, 1]),
+            pltpu.make_async_copy(wd.at[k], out_down.at[0, :, at], o_sem.at[k, 2]),
         )
 
     def weight_grads(k):
-        rows = pl.ds(pl.multiple_of(k * LANES, LANES), LANES)
-        both = dot_tn(xc[k, 0], gsus[...]).astype(BF)
-        stg[rows, 0:256] = both[:, 0:256]
-        stu[rows, 0:256] = both[:, 256:512]
-        stg[rows, 256:hid] = both[:, 512:512 + rest]
-        stu[rows, 256:hid] = both[:, 640:640 + rest]
+        for m in range(3):
+            rows = pl.ds(m * 256, 256)
+            wc[k, rows, :] = dot_nn(gsus_t[rows, :], xc[k, 0]).astype(BF)
         wd[k] = dot_nn(hid_t[:hid], xc[k, 1]).astype(BF)
         for cp in out_copies(k):
             cp.start()
@@ -431,10 +425,10 @@
             def _():
                 stage(n, True, n - 1)
 
-        @pl.when(t < nc)
+        @pl.when((t >= 1) & (t <= nc))
         def _():
-            weight_grads(2 * t)
-            weight_grads(2 * t + 1)
+            weight_grads(core * nc + t - 1)
+            weight_grads((1 - core) * nc + t - 1)
 
         return carry
 
@@ -531,8 +525,8 @@
         out_shape=(
             jax.ShapeDtypeStruct((rows, half), BF),
             jax.ShapeDtypeStruct((ROWS, 128), F32),
-            jax.ShapeDtypeStruct(gate_weight.shape, BF),
-            jax.ShapeDtypeStruct(up_weight.shape, BF),
+            jax.ShapeDtypeStruct((1, hid, width), BF),
+            jax.ShapeDtypeStruct((1, hid, width), BF),
             jax.ShapeDtypeStruct(down_weight.shape, BF),
         ),
         in_specs=[
@@ -557,14 +551,13 @@
             vmem((128, 128), BF),
             vmem((3, 128, 128), BF),
             vmem((2 * BUNDLE, 128), F32),
-            vmem((width, hid), BF),
-            vmem((width, hid), BF),
             vmem((2 * nc, hid, LANES), BF),
-            vmem((2 * nc, LANES, 768), BF),
-            vmem((slots, 768), F32),
-            vmem((slots, 384), F32),
-            vmem((slots, 768), BF),
-            vmem((384, slots), BF),
+            vmem((2 * nc, 2 * SIDE_HID, LANES), BF),
+            vmem((slots, 2 * SIDE_HID), F32),
+            vmem((slots, SIDE_HID), F32),
+            vmem((slots, 2 * SIDE_HID), BF),
+            vmem((2 * SIDE_HID, slots), BF),
+            vmem((SIDE_HID, slots), BF),
             vmem((2, slots, LANES), F32),
             vmem((nc, slots, LANES), BF),
             vmem((nc, slots, LANES), BF),
@@ -572,7 +565,7 @@
             vmem((slots, 128), BF),
             vmem((slots, 128), BF),
             *chunk_buffers((), 128),
-            dma((2 + 2 * nc,)),
+            dma((2 * nc, 3)),
             dma((nc + 1, 3)), dma((nc + 1, 3)),
             dma((nc, 3)), dma((nc, 3)),
             dma((nc, 4)), dma((nc, 4)),
@@ -587,9 +580,9 @@
         compiler_params=pltpu.CompilerParams(
             collective_id=0, has_side_effects=True, vmem_limit_bytes=63 * 1024 * 1024
         ),
-    )(src, info, gate_weight, up_weight, down_weight)
+    )(src, info, gate_weight.transpose(0, 2, 1), up_weight.transpose(0, 2, 1), down_weight)
     route_grad = shares[:rows, :TOP] / route_weights
-    return token_grad, route_grad, gate_grad, up_grad, down_grad
+    return token_grad, route_grad, gate_grad.transpose(0, 2, 1), up_grad.transpose(0, 2, 1), down_grad
 
 
 def solution(mesh):

time: 152 us -> 143 us (0.941)
  local copies, waits for them, and re-layouts: 21.6 us -> 12.7 us
    unnamed x19 -> x11, local copies, waits for them, and re-layouts: 20.1 us -> 11.2 us
where the time goes in v2:
time: 143 us; the launch traced here: 142 us
  Pallas kernels  125 us (87%)
  local copies, waits for them, and re-layouts  12.7 us (9%)
  other arithmetic  4.11 us (3%)
    pallas_call x1, Pallas kernels, per_device(): pl.pallas_call(functools.partial(kernel, nc, hid), out_shape=(jax.ShapeDt...  125 us
    unnamed x11, local copies, waits for them, and re-layouts  11.2 us

profile of v2, /device:TPU:0, one launch (start us, length us, event | category | flops | bytes accessed | tf_op | source)
XLA Modules:
  0.0 142.4 jit_solution(12378604256722516499)
XLA Ops:
  0.7 0.1 broadcast_in_dim.52
  0.7 0.1 broadcast_in_dim.53
  0.8 0.8 fusion
  1.6 0.1 copy.44
  1.7 0.5 convert_reduce_fusion
  2.2 0.1 copy.39
  2.3 0.1 copy.40
  2.3 0.8 select_reduce_fusion
  3.1 0.1 copy.41
  3.2 0.8 copy.42
  4.0 0.1 broadcast_in_dim.59
  4.1 0.6 broadcast_select_fusion.info
  4.7 1.0 constant_dynamic-slice_fusion
  5.7 0.7 pad_maximum_fusion.src
  6.4 124.9 %shard_map.110 = (bf16[24,2048]{1,0:T(8,128)(2,1)}, f32[32,128]{1,0:T(8,128)}, bf16[1,344,4096]{2,1,0:T(8,128)(2,1)}, bf16[1,344,4096]{2,1,0:T(8,128)(2,1)}, bf16[1,344,4096]{2,1,0:T(8,128)(2,1)}) custom-call(bf16[8,2,32,256]{3,2,1,0:T(8,128)(2,1)} %pad_maximum_fusion.src, f32[3,8,128]{2,1,0:T(8,128)} %broadcast_select_fusion.info, ...), custom_call_target="tpu_custom_call" | custom-call | tf_op jit(solution)/shard_map/pallas_call | solution.py:523
  131.3 0.7 slice_divide_fusion
  132.0 0.6 copy.43
  132.7 1.5 %copy.55 = bf16[24,2048]{1,0:T(8,128)(2,1)} copy(bf16[24,2048]{1,0:T(8,128)(2,1)} %get-tuple-element.56) | data formatting | bytes 196608
  134.2 0.0 copy-start.1
  134.2 3.8 %copy.56 = bf16[1,4096,344]{1,2,0:T(8,128)(2,1)} copy(bf16[1,4096,344]{1,2,0:T(8,128)(2,1)} %bitcast.39) | data formatting | bytes 5636096
  138.0 0.0 copy-done.1
  138.0 1.6 %copy.57 = bf16[1,4096,344]{1,2,0:T(8,128)(2,1)} copy(bf16[1,4096,344]{1,2,0:T(8,128)(2,1)S(1)} %bitcast.38) | data formatting | bytes 5636096
  139.6 1.3 copy-done
  140.8 1.6 %copy.58 = bf16[1,344,4096]{2,1,0:T(8,128)(2,1)} copy(bf16[1,344,4096]{2,1,0:T(8,128)(2,1)S(1)} %copy-done) | data formatting | bytes 5636096
  (11 shorter events, 0.1 us)
Async XLA Ops:
  134.2 3.8 %copy-start.1 = (bf16[1,344,4096]{2,1,0:T(8,128)(2,1)S(1)}, bf16[1,344,4096]{2,1,0:T(8,128)(2,1)}, u32[]{:S(2)}) copy-start(bf16[1,344,4096]{2,1,0:T(8,128)(2,1)} %get-tuple-element.13) | copy-start | bytes 8454148
  138.0 2.8 %copy-start = (bf16[1,344,4096]{2,1,0:T(8,128)(2,1)S(1)}, bf16[1,344,4096]{2,1,0:T(8,128)(2,1)}, u32[]{:S(2)}) copy-start(bf16[1,344,4096]{2,1,0:T(8,128)(2,1)} %get-tuple-element.60) | copy-start | bytes 8454148

commit v3 on v2

--- a/solution.py
+++ b/solution.py
@@ -14,6 +14,7 @@
 ROWS = 32
 BUNDLE = 48
 LANES = 256
+AHEAD = 3
 SIDE_HID = 384
 BF = jnp.bfloat16
 F32 = jnp.float32
@@ -34,13 +35,13 @@
 
 def kernel(
     nc, hid,
-    src, info, gate, up, down,
+    tokens, cotangent, routes, weights, gate, up, down,
     out_tok, out_rg, out_gate, out_up, out_down,
-    tz, iz, xc, ob, place, place_t, share,
+    tz, info, iz, codes, xc, ob, place, place_t, share,
     wd, wc, pre, hg, gsus, gsus_t, hid_t,
     part, tps, tpr, s_f, xa_f, xb_f, yr_f, zs_f, zr_f,
     part_r, tpr_r, s_r, xa_r, xb_r, yr_r, zs_r, zr_r,
-    w_sem, z_send, z_recv, y_send, y_recv, x_send, x_recv, d_send, d_recv,
+    w_sem, own_sem, z_send, z_recv, i_send, i_recv, y_send, y_recv, x_send, x_recv, p_send, p_recv, d_send, d_recv,
     e_send, e_recv, a_send, a_recv, b_send, b_recv, v_send, v_recv, q_send, q_recv,
     o_sem,
 ):
@@ -60,6 +61,18 @@
     cross2_y = 2 * (1 - pair) + y % 2
     y_peers = [partner_y, cross_y, cross2_y]
     z_peers = [(z + 1) % 4, (z + 3) % 4, (z + 2) % 4]
+
+    rows_dev = tokens.shape[0]
+    half_of = ((y + 1) // 2) % 2
+
+    def block(xs, ys):
+        return xs * 192 + (((ys + 1) // 2) % 2) * 96 + (ys // 2) * BUNDLE
+
+    def pad_rows(c, carry):
+        tz[c, :, :, rows_dev:, :] = jnp.zeros((SIDE, 2, ROWS - rows_dev, LANES), BF)
+        return carry
+
+    lax.fori_loop(0, nc, pad_rows, 0)
 
     barrier = pltpu.get_barrier_semaphore()
     for zz in z_peers:
@@ -87,39 +100,68 @@
             src_ref=a, dst_ref=b, send_sem=ss, recv_sem=rs, device_id=dev, device_id_type=MESH
         )
 
-    def z_copy(c, i):
+    def piece(ref, c):
+        return ref.at[:, pl.ds(pl.multiple_of((core * nc + c) * LANES, LANES), LANES)]
+
+    def landing(c, tensor):
+        return tz.at[c, z, tensor, pl.ds(0, rows_dev)]
+
+    def z_copy(c, i, tensor):
         return remote(
-            src.at[c], tz.at[c, z], z_send.at[c, i], z_recv.at[c, i], chip(z_peers[i], y, x)
+            piece(cotangent if tensor else tokens, c), landing(c, tensor),
+            z_send.at[c, i, tensor], z_recv.at[c, i, tensor], chip(z_peers[i], y, x),
+        )
+
+    def own_copy(c, tensor):
+        return pltpu.make_async_copy(
+            piece(cotangent if tensor else tokens, c), landing(c, tensor), own_sem.at[c, tensor]
         )
 
     def zi_copy(i):
-        return remote(
-            info, iz.at[i + 1], z_send.at[nc, i], z_recv.at[nc, i], chip(z_peers[i], y, x)
-        )
-
+        return remote(info, iz.at[z], i_send.at[i], i_recv.at[i], chip(z_peers[i], y, x))
+
+    def start_z(c):
+        for tensor in range(2):
+            for i in range(3):
+                z_copy(c, i, tensor).start()
+            own_copy(c, tensor).start()
+
+    start_z(0)
+
+    expert_row = lax.broadcasted_iota(jnp.int32, (EXPERTS, rows_dev), 0)
+    hot = [expert_row == routes[k:k + 1, :] for k in range(2)]
+    hit = jnp.where(hot[0] | hot[1], 1.0, 0.0).astype(BF)
+    before = jnp.where(
+        lax.broadcasted_iota(jnp.int32, (rows_dev, rows_dev), 0)
+        < lax.broadcasted_iota(jnp.int32, (rows_dev, rows_dev), 1),
+        1.0, 0.0,
+    ).astype(BF)
+    code = dot_nn(hit, before) + (z * CAP + 1).astype(F32)
+    info[...] = jnp.zeros_like(info)
+    for k in range(2):
+        info[k, :, 0:rows_dev] = jnp.where(hot[k], code, 0.0)
+    info[2, :, 0:rows_dev] = jnp.where(hot[0], weights[0:1, :], 0.0) + jnp.where(
+        hot[1], weights[1:2, :], 0.0
+    )
     for i in range(3):
         zi_copy(i).start()
-
-    def start_z(c, carry):
-        for i in range(3):
-            z_copy(c, i).start()
-        return carry
-
-    lax.fori_loop(0, nc, start_z, 0)
-
-    iz[0] = info[...]
+    for c in range(1, AHEAD):
+        start_z(c)
+    iz[z] = info[...]
     pre[...] = jnp.zeros_like(pre)
     hg[...] = jnp.zeros_like(hg)
     for i in range(3):
         zi_copy(i).wait_recv()
+    for kind in range(3):
+        total = iz[0, kind]
+        for zz in range(1, SIDE):
+            total = total + pltpu.roll(iz[zz, kind], zz * ROWS, 1)
+        codes[kind] = total
 
     slot_number = lax.broadcasted_iota(jnp.int32, (BUNDLE, 128), 0).astype(F32) + 1.0
 
     def info_row(kind, expert):
-        total = iz[0, kind, pl.ds(expert, 1), :]
-        for i in range(1, 4):
-            total = total + iz[i, kind, pl.ds(expert, 1), :]
-        return total
+        return codes[kind, pl.ds(expert, 1), :]
 
     spare = jnp.zeros((128 - 2 * BUNDLE, 128), F32)
     first, second = [], []
@@ -139,66 +181,60 @@
 
     def y_copy(c, i):
         k = core * nc + c
-        at = pl.ds(x * 192 + y * BUNDLE, BUNDLE)
-        from_ref = xc.at[k, :, at, :] if i == 0 else ob.at[c]
+        at = pl.ds(block(x, y), BUNDLE)
+        tensor = 1 if i == 3 else 0
+        peer = cross_y if i == 3 else y_peers[i]
+        from_ref = xc.at[k, 0, at, :] if i == 0 else ob.at[c, tensor]
         return remote(
-            from_ref, xc.at[k, :, at, :], y_send.at[c, i], y_recv.at[c, i],
-            chip(z, y_peers[i], x),
-        )
-
-    def y_arrival(c, i):
-        k = core * nc + c
-        at = pl.ds(x * 192 + y_peers[i] * BUNDLE, BUNDLE)
-        return remote(
-            ob.at[c], xc.at[k, :, at, :], y_send.at[c, i], y_recv.at[c, i],
-            chip(z, y_peers[i], x),
+            from_ref, xc.at[k, tensor, at, :], y_send.at[c, i], y_recv.at[c, i], chip(z, peer, x)
         )
 
     def x_copy(c, i):
         k = core * nc + c
-        if i < 2:
-            at = pl.ds(x * 192, 192)
-        elif i == 2:
-            at = pl.ds(((x + 3) % 4) * 192, 96)
+        tensor = i // 4
+        step = i % 4
+        size, base = (96, half_of * 96) if tensor else (192, 0)
+        if step < 2:
+            at = pl.ds(x * 192 + base, size)
+        elif step == 2:
+            at = pl.ds(((x + 3) % 4) * 192 + base, size // 2)
         else:
-            at = pl.ds(((x + 1) % 4) * 192 + 96, 96)
+            at = pl.ds(((x + 1) % 4) * 192 + base + size // 2, size // 2)
+        ref = xc.at[k, tensor, at, :]
         return remote(
-            xc.at[k, :, at, :], xc.at[k, :, at, :], x_send.at[c, i], x_recv.at[c, i],
-            right if i % 2 == 0 else left,
-        )
-
-    def x_arrival(c, i):
+            ref, ref, x_send.at[c, i], x_recv.at[c, i], right if i % 2 == 0 else left
+        )
+
+    def p_copy(c, i):
+        at = pl.ds(((x + (0, 3, 1, 2)[i]) % 4) * 192 + half_of * 96, 96)
+        ref = xc.at[core * nc + c, 1, at, :]
+        return remote(ref, ref, p_send.at[c, i], p_recv.at[c, i], chip(z, partner_y, x))
+
+    def d_copy(c, k, tensor):
+        ref = xc.at[k, tensor]
+        return remote(ref, ref, d_send.at[c, tensor], d_recv.at[c, tensor], other_core)
+
+    def compact(c):
+        for tensor in range(2):
+            for i in range(3):
+                z_copy(c, i, tensor).wait_recv()
+            own_copy(c, tensor).wait()
+
+        @pl.when(c + AHEAD < nc)
+        def _():
+            start_z(c + AHEAD)
+
         k = core * nc + c
-        if i == 0:
-            at = pl.ds(((x + 3) % 4) * 192, 192)
-        elif i == 1:
-            at = pl.ds(((x + 1) % 4) * 192, 192)
-        elif i == 2:
-            at = pl.ds(((x + 2) % 4) * 192, 96)
-        else:
-            at = pl.ds(((x + 2) % 4) * 192 + 96, 96)
-        return remote(
-            xc.at[k, :, at, :], xc.at[k, :, at, :], x_send.at[c, i], x_recv.at[c, i],
-            right if i % 2 == 0 else left,
-        )
-
-    def d_copy(c, k):
-        return remote(xc.at[k], xc.at[k], d_send.at[c], d_recv.at[c], other_core)
-
-    def compact(c):
-        for i in range(3):
-            z_copy(c, i).wait_recv()
-        k = core * nc + c
-        at = pl.ds(pl.multiple_of(x * 192 + y * BUNDLE, BUNDLE), BUNDLE)
-        for tensor in range(2):
+        at = pl.ds(pl.multiple_of(block(x, y), BUNDLE), BUNDLE)
+        for tensor in (1, 0):
             rows = dot_nn(place[:2 * BUNDLE], tz[c, :, tensor].reshape(SIDE * ROWS, LANES))
             if tensor == 1:
                 rows = rows * share[:, 0:1]
             rows = rows.astype(BF)
             xc[k, tensor, at, :] = rows[:BUNDLE]
             ob[c, tensor] = rows[BUNDLE:]
-        for i in range(3):
-            y_copy(c, i).start()
+            for i in ((3,) if tensor else (0, 1, 2)):
+                y_copy(c, i).start()
 
     def products(k):
         for m in range(3):
@@ -220,10 +256,15 @@
 
         @pl.when((t >= 1) & (t < nc + 1))
         def _():
+            c = t - 1
+            y_copy(c, 3).wait_recv()
+            x_copy(c, 4).start()
+            x_copy(c, 5).start()
+            p_copy(c, 0).start()
             for i in range(3):
-                y_arrival(t - 1, i).wait_recv()
-            for i in range(2):
-                x_copy(t - 1, i).start()
+                y_copy(c, i).wait_recv()
+            x_copy(c, 0).start()
+            x_copy(c, 1).start()
 
         @pl.when(t == 1)
         def _():
@@ -232,31 +273,43 @@
 
         @pl.when((t >= 2) & (t < nc + 2))
         def _():
-            for i in range(2):
-                x_arrival(t - 2, i).wait_recv()
-            for i in range(2, 4):
-                x_copy(t - 2, i).start()
+            c = t - 2
+            for side in range(2):
+                x_copy(c, 4 + side).wait_recv()
+                x_copy(c, 6 + side).start()
+                p_copy(c, 1 + side).start()
+            for side in range(2):
+                x_copy(c, side).wait_recv()
+                x_copy(c, 2 + side).start()
 
         @pl.when((t >= 3) & (t < nc + 3))
         def _():
-            for i in range(2, 4):
-                x_arrival(t - 3, i).wait_recv()
-            d_copy(t - 3, core * nc + t - 3).start()
-            products(core * nc + t - 3)
-
-        @pl.when(t >= 4)
-        def _():
-            d_copy(t - 4, (1 - core) * nc + t - 4).wait_recv()
-            products((1 - core) * nc + t - 4)
-
-        return carry
-
-    def own_rows(c, carry):
-        tz[c, z] = src[c]
-        return carry
-
-    lax.fori_loop(0, nc, own_rows, 0)
-    lax.fori_loop(0, nc + 4, dispatch, 0)
+            c = t - 3
+            for side in range(2):
+                x_copy(c, 6 + side).wait_recv()
+            p_copy(c, 3).start()
+            for side in range(2):
+                x_copy(c, 2 + side).wait_recv()
+            d_copy(c, core * nc + c, 0).start()
+
+        @pl.when((t >= 4) & (t < nc + 4))
+        def _():
+            c = t - 4
+            for i in range(4):
+                p_copy(c, i).wait_recv()
+            d_copy(c, core * nc + c, 1).start()
+            products(core * nc + c)
+
+        @pl.when(t >= 5)
+        def _():
+            c = t - 5
+            for tensor in range(2):
+                d_copy(c, (1 - core) * nc + c, tensor).wait_recv()
+            products((1 - core) * nc + c)
+
+        return carry
+
+    lax.fori_loop(0, nc + 5, dispatch, 0)
 
     def gates(m, carry):
         rows = pl.ds(pl.multiple_of(m * 128, 128), 128)
@@ -305,7 +358,7 @@
 
     def v_copy(n, feature, c, i):
         s, yr = pick(feature, c, s_f, s_r), pick(feature, c, yr_f, yr_r)
-        at = pl.ds(x * 192 + y_peers[i] * BUNDLE, BUNDLE)
+        at = pl.ds(block(x, y_peers[i]), BUNDLE)
         return remote(
             s.at[at], yr.at[i], v_send.at[n, i], v_recv.at[n, i], chip(z, y_peers[i], x)
         )
@@ -364,7 +417,7 @@
         zs = pick(feature, c, zs_f, zs_r)
         for i in range(3):
             v_copy(n, feature, c, i).wait_recv()
-        at = pl.ds(pl.multiple_of(x * 192 + y * BUNDLE, BUNDLE), BUNDLE)
+        at = pl.ds(pl.multiple_of(block(x, y), BUNDLE), BUNDLE)
         mine = (s[at, :].astype(F32) + yr[0].astype(F32)).astype(BF)
         theirs = (yr[1].astype(F32) + yr[2].astype(F32)).astype(BF)
         slots = jnp.concatenate(
@@ -393,7 +446,8 @@
         if feature:
             out_tok[:, pl.ds(pl.multiple_of(c * LANES, LANES), LANES)] = total[:24].astype(BF)
         else:
-            out_rg[...] = total
+            turned = jnp.concatenate([total, jnp.zeros((128 - ROWS, 128), F32)], axis=0).T
+            out_rg[...] = turned[0:TOP, 0:rows_dev] / weights[...]
 
     def out_copies(k):
         at = pl.ds(pl.multiple_of(k * LANES, LANES), LANES)
@@ -439,11 +493,15 @@
 
     def drain_dispatch(c, carry):
         for i in range(3):
-            z_copy(c, i).wait_send()
+            for tensor in range(2):
+                z_copy(c, i, tensor).wait_send()
+        for i in range(4):
             y_copy(c, i).wait_send()
-        for i in range(4):
+            p_copy(c, i).wait_send()
+        for i in range(8):
             x_copy(c, i).wait_send()
-        d_copy(c, core * nc + c).wait_send()
+        for tensor in range(2):
+            d_copy(c, core * nc + c, tensor).wait_send()
         return carry
 
     lax.fori_loop(0, nc, drain_dispatch, 0)
@@ -474,38 +532,10 @@
 
 
 def per_device(tokens, cotangent, routes, route_weights, gate_weight, up_weight, down_weight):
-    ep = lax.axis_index("ep")
-    core = lax.axis_index("tp")
-    z = ep // 16
     rows, width = tokens.shape
     half = width // lax.axis_size("tp")
     nc = half // LANES
     hid = gate_weight.shape[2]
-
-    def halves(a):
-        piece = lax.dynamic_slice_in_dim(a, core * half, half, 1)
-        piece = jnp.pad(piece, ((0, ROWS - rows), (0, 0)))
-        return piece.reshape(ROWS, nc, LANES).transpose(1, 0, 2)
-
-    src = jnp.stack([halves(tokens), halves(cotangent)], axis=1)
-
-    hot = routes[:, :, None] == jnp.arange(EXPERTS, dtype=jnp.int32)[None, None, :]
-    hit = jnp.any(hot, axis=1)
-    earlier = jnp.arange(rows)[:, None] > jnp.arange(rows)[None, :]
-    position = jnp.sum((earlier[:, :, None] & hit[None, :, :]).astype(jnp.int32), axis=1)
-    code = (position + z * CAP + 1).astype(F32)
-    kinds = jnp.stack(
-        [
-            jnp.where(hot[:, 0], code, 0.0),
-            jnp.where(hot[:, 1], code, 0.0),
-            jnp.sum(jnp.where(hot, route_weights[:, :, None], 0.0), axis=1),
-        ]
-    )
-    info = jnp.pad(kinds.transpose(0, 2, 1), ((0, 0), (0, 0), (0, ROWS - rows)))
-    column = jnp.arange(SIDE, dtype=jnp.int32) == z
-    info = jnp.where(column[None, None, :, None], info[:, :, None, :], 0.0)
-    info = info.reshape(3, EXPERTS, SIDE * ROWS)
-
     vmem, anywhere = pltpu.VMEM, pl.ANY
     slots = 16 * BUNDLE
 
@@ -524,12 +554,14 @@
         functools.partial(kernel, nc, hid),
         out_shape=(
             jax.ShapeDtypeStruct((rows, half), BF),
-            jax.ShapeDtypeStruct((ROWS, 128), F32),
+            jax.ShapeDtypeStruct((TOP, rows), F32),
             jax.ShapeDtypeStruct((1, hid, width), BF),
             jax.ShapeDtypeStruct((1, hid, width), BF),
             jax.ShapeDtypeStruct(down_weight.shape, BF),
         ),
         in_specs=[
+            pl.BlockSpec(memory_space=anywhere),
+            pl.BlockSpec(memory_space=anywhere),
             pl.BlockSpec(memory_space=vmem),
             pl.BlockSpec(memory_space=vmem),
             pl.BlockSpec(memory_space=anywhere),
@@ -545,7 +577,9 @@
         ),
         scratch_shapes=[
             vmem((nc, SIDE, 2, ROWS, LANES), BF),
+            vmem((3, EXPERTS, 128), F32),
             vmem((SIDE, 3, EXPERTS, 128), F32),
+            vmem((3, EXPERTS, 128), F32),
             vmem((2 * nc, 2, slots, LANES), BF),
             vmem((nc, 2, BUNDLE, LANES), BF),
             vmem((128, 128), BF),
@@ -566,10 +600,13 @@
             vmem((slots, 128), BF),
             *chunk_buffers((), 128),
             dma((2 * nc, 3)),
-            dma((nc + 1, 3)), dma((nc + 1, 3)),
-            dma((nc, 3)), dma((nc, 3)),
+            dma((nc, 2)),
+            dma((nc, 3, 2)), dma((nc, 3, 2)),
+            dma((3,)), dma((3,)),
             dma((nc, 4)), dma((nc, 4)),
-            dma((nc,)), dma((nc,)),
+            dma((nc, 8)), dma((nc, 8)),
+            dma((nc, 4)), dma((nc, 4)),
+            dma((nc, 2)), dma((nc, 2)),
             dma((nc + 1,)), dma((nc + 1,)),
             dma((nc + 1, 2)), dma((nc + 1, 2)),
             dma((nc + 1, 2)), dma((nc + 1, 2)),
@@ -580,9 +617,11 @@
         compiler_params=pltpu.CompilerParams(
             collective_id=0, has_side_effects=True, vmem_limit_bytes=63 * 1024 * 1024
         ),
-    )(src, info, gate_weight.transpose(0, 2, 1), up_weight.transpose(0, 2, 1), down_weight)
-    route_grad = shares[:rows, :TOP] / route_weights
-    return token_grad, route_grad, gate_grad.transpose(0, 2, 1), up_grad.transpose(0, 2, 1), down_grad
+    )(
+        tokens, cotangent, routes.T, route_weights.T,
+        gate_weight.transpose(0, 2, 1), up_weight.transpose(0, 2, 1), down_weight,
+    )
+    return token_grad, shares.T, gate_grad.transpose(0, 2, 1), up_grad.transpose(0, 2, 1), down_grad
 
 
 def solution(mesh):

time: 143 us -> 129 us (0.902)
  Pallas kernels: 125 us -> 117 us
  other arithmetic: 4.11 us -> 0 us
  local copies, waits for them, and re-layouts: 12.7 us -> 11 us
    pallas_call x1, Pallas kernels: 125 us -> 117 us  [per_device(): pl.pallas_call(functools.partial(kernel, nc, hid), out_shape=(jax.ShapeDt...]
    unnamed x11 -> x9, local copies, waits for them, and re-layouts: 11.2 us -> 11 us
where the time goes in v3:
time: 129 us; the launch traced here: 128 us
  Pallas kernels  117 us (91%)
  local copies, waits for them, and re-layouts  11 us (9%)
    pallas_call x1, Pallas kernels, per_device(): pl.pallas_call(functools.partial(kernel, nc, hid), out_shape=(jax.ShapeDt...  117 us
    unnamed x9, local copies, waits for them, and re-layouts  11 us

profile of v3, /device:TPU:0, one launch (start us, length us, event | category | flops | bytes accessed | tf_op | source)
XLA Modules:
  0.0 128.4 jit_solution(13926977162418442278)
XLA Ops:
  0.6 116.8 %shard_map.110 = (bf16[24,2048]{1,0:T(8,128)(2,1)}, f32[2,24]{1,0:T(2,128)}, bf16[1,344,4096]{2,1,0:T(8,128)(2,1)}, bf16[1,344,4096]{2,1,0:T(8,128)(2,1)}, bf16[1,344,4096]{2,1,0:T(8,128)(2,1)}) custom-call(bf16[24,4096]{1,0:T(8,128)(2,1)} %tokens.1, bf16[24,4096]{1,0:T(8,128)(2,1)} %cotangent.1, s32[2,24]{1,0:T(2,128)} %bitcast.11, f32[2,24]{1,0:T(2,128)} %bitcast.12, ...), custom_call_target="tpu_custom_call" | custom-call | tf_op jit(solution)/shard_map/pallas_call | solution.py:553
  117.5 1.5 %copy.17 = bf16[24,2048]{1,0:T(8,128)(2,1)} copy(bf16[24,2048]{1,0:T(8,128)(2,1)} %get-tuple-element.20) | data formatting | bytes 196608
  119.0 1.2 copy.18
  120.2 0.0 copy-start.1
  120.2 3.8 %copy.19 = bf16[1,4096,344]{1,2,0:T(8,128)(2,1)} copy(bf16[1,4096,344]{1,2,0:T(8,128)(2,1)} %bitcast.10) | data formatting | bytes 5636096
  124.0 0.0 copy-done.1
  124.1 0.0 copy-start
  124.1 1.6 %copy.20 = bf16[1,4096,344]{1,2,0:T(8,128)(2,1)} copy(bf16[1,4096,344]{1,2,0:T(8,128)(2,1)S(1)} %bitcast.9) | data formatting | bytes 5636096
  125.6 1.3 copy-done
  126.9 1.6 %copy.21 = bf16[1,344,4096]{2,1,0:T(8,128)(2,1)} copy(bf16[1,344,4096]{2,1,0:T(8,128)(2,1)S(1)} %copy-done) | data formatting | bytes 5636096
Async XLA Ops:
  120.2 3.8 %copy-start.1 = (bf16[1,344,4096]{2,1,0:T(8,128)(2,1)S(1)}, bf16[1,344,4096]{2,1,0:T(8,128)(2,1)}, u32[]{:S(2)}) copy-start(bf16[1,344,4096]{2,1,0:T(8,128)(2,1)} %get-tuple-element.13) | copy-start | bytes 8454148
  124.1 2.8 %copy-start = (bf16[1,344,4096]{2,1,0:T(8,128)(2,1)S(1)}, bf16[1,344,4096]{2,1,0:T(8,128)(2,1)}, u32[]{:S(2)}) copy-start(bf16[1,344,4096]{2,1,0:T(8,128)(2,1)} %get-tuple-element.24) | copy-start | bytes 8454148

commit v4 on v3

--- a/solution.py
+++ b/solution.py
@@ -39,9 +39,9 @@
     out_tok, out_rg, out_gate, out_up, out_down,
     tz, info, iz, codes, xc, ob, place, place_t, share,
     wd, wc, pre, hg, gsus, gsus_t, hid_t,
-    part, tps, tpr, s_f, xa_f, xb_f, yr_f, zs_f, zr_f,
+    s_f, tpr, xa_f, xb_f, yr_f, zs_f, zr_f,
     part_r, tpr_r, s_r, xa_r, xb_r, yr_r, zs_r, zr_r,
-    w_sem, own_sem, z_send, z_recv, i_send, i_recv, y_send, y_recv, x_send, x_recv, p_send, p_recv, d_send, d_recv,
+    w_sem, z_send, z_recv, i_send, i_recv, y_send, y_recv, x_send, x_recv, p_send, p_recv, d_send, d_recv,
     e_send, e_recv, a_send, a_recv, b_send, b_recv, v_send, v_recv, q_send, q_recv,
     o_sem,
 ):
@@ -86,9 +86,9 @@
     for k in range(2 * nc):
         at = pl.ds(k * LANES, LANES)
         w_copies += [
-            pltpu.make_async_copy(gate.at[0, :, at], wc.at[k, pl.ds(0, hid)], w_sem.at[k, 0]),
-            pltpu.make_async_copy(up.at[0, :, at], wc.at[k, pl.ds(SIDE_HID, hid)], w_sem.at[k, 1]),
-            pltpu.make_async_copy(down.at[0, :, at], wd.at[k], w_sem.at[k, 2]),
+            pltpu.make_async_copy(gate.at[0, :, at], wc.at[k, pl.ds(0, hid)], w_sem.at[0]),
+            pltpu.make_async_copy(up.at[0, :, at], wc.at[k, pl.ds(SIDE_HID, hid)], w_sem.at[1]),
+            pltpu.make_async_copy(down.at[0, :, at], wd.at[k], w_sem.at[2]),
         ]
     for cp in w_copies:
         cp.start()
@@ -100,6 +100,12 @@
             src_ref=a, dst_ref=b, send_sem=ss, recv_sem=rs, device_id=dev, device_id_type=MESH
         )
 
+    def settle(ref, sem):
+        pltpu.make_async_copy(ref, ref, sem).wait()
+
+    def some(n):
+        return xc.at[0, 0, pl.ds(0, n)]
+
     def piece(ref, c):
         return ref.at[:, pl.ds(pl.multiple_of((core * nc + c) * LANES, LANES), LANES)]
 
@@ -109,16 +115,16 @@
     def z_copy(c, i, tensor):
         return remote(
             piece(cotangent if tensor else tokens, c), landing(c, tensor),
-            z_send.at[c, i, tensor], z_recv.at[c, i, tensor], chip(z_peers[i], y, x),
+            z_send.at[0], z_recv.at[c], chip(z_peers[i], y, x),
         )
 
     def own_copy(c, tensor):
         return pltpu.make_async_copy(
-            piece(cotangent if tensor else tokens, c), landing(c, tensor), own_sem.at[c, tensor]
+            piece(cotangent if tensor else tokens, c), landing(c, tensor), z_recv.at[c]
         )
 
     def zi_copy(i):
-        return remote(info, iz.at[z], i_send.at[i], i_recv.at[i], chip(z_peers[i], y, x))
+        return remote(info, iz.at[z], i_send.at[0], i_recv.at[0], chip(z_peers[i], y, x))
 
     def start_z(c):
         for tensor in range(2):
@@ -150,8 +156,7 @@
     iz[z] = info[...]
     pre[...] = jnp.zeros_like(pre)
     hg[...] = jnp.zeros_like(hg)
-    for i in range(3):
-        zi_copy(i).wait_recv()
+    settle(iz.at[pl.ds(0, 3)], i_recv.at[0])
     for kind in range(3):
         total = iz[0, kind]
         for zz in range(1, SIDE):
@@ -186,7 +191,7 @@
         peer = cross_y if i == 3 else y_peers[i]
         from_ref = xc.at[k, 0, at, :] if i == 0 else ob.at[c, tensor]
         return remote(
-            from_ref, xc.at[k, tensor, at, :], y_send.at[c, i], y_recv.at[c, i], chip(z, peer, x)
+            from_ref, xc.at[k, tensor, at, :], y_send.at[0], y_recv.at[c, tensor], chip(z, peer, x)
         )
 
     def x_copy(c, i):
@@ -202,23 +207,20 @@
             at = pl.ds(((x + 1) % 4) * 192 + base + size // 2, size // 2)
         ref = xc.at[k, tensor, at, :]
         return remote(
-            ref, ref, x_send.at[c, i], x_recv.at[c, i], right if i % 2 == 0 else left
+            ref, ref, x_send.at[i // 2], x_recv.at[c, i // 2], right if i % 2 == 0 else left
         )
 
     def p_copy(c, i):
         at = pl.ds(((x + (0, 3, 1, 2)[i]) % 4) * 192 + half_of * 96, 96)
         ref = xc.at[core * nc + c, 1, at, :]
-        return remote(ref, ref, p_send.at[c, i], p_recv.at[c, i], chip(z, partner_y, x))
+        return remote(ref, ref, p_send.at[0], p_recv.at[c], chip(z, partner_y, x))
 
     def d_copy(c, k, tensor):
         ref = xc.at[k, tensor]
-        return remote(ref, ref, d_send.at[c, tensor], d_recv.at[c, tensor], other_core)
+        return remote(ref, ref, d_send.at[0], d_recv.at[c], other_core)
 
     def compact(c):
-        for tensor in range(2):
-            for i in range(3):
-                z_copy(c, i, tensor).wait_recv()
-            own_copy(c, tensor).wait()
+        settle(some(8 * rows_dev), z_recv.at[c])
 
         @pl.when(c + AHEAD < nc)
         def _():
@@ -257,54 +259,50 @@
         @pl.when((t >= 1) & (t < nc + 1))
         def _():
             c = t - 1
-            y_copy(c, 3).wait_recv()
+            settle(some(BUNDLE), y_recv.at[c, 1])
             x_copy(c, 4).start()
             x_copy(c, 5).start()
             p_copy(c, 0).start()
-            for i in range(3):
-                y_copy(c, i).wait_recv()
+            settle(some(3 * BUNDLE), y_recv.at[c, 0])
             x_copy(c, 0).start()
             x_copy(c, 1).start()
 
         @pl.when(t == 1)
         def _():
-            for cp in w_copies:
-                cp.wait()
+            settle(gate.at[0], w_sem.at[0])
+            settle(up.at[0], w_sem.at[1])
+            settle(down.at[0], w_sem.at[2])
 
         @pl.when((t >= 2) & (t < nc + 2))
         def _():
             c = t - 2
+            settle(some(192), x_recv.at[c, 2])
             for side in range(2):
-                x_copy(c, 4 + side).wait_recv()
                 x_copy(c, 6 + side).start()
                 p_copy(c, 1 + side).start()
+            settle(some(384), x_recv.at[c, 0])
             for side in range(2):
-                x_copy(c, side).wait_recv()
                 x_copy(c, 2 + side).start()
 
         @pl.when((t >= 3) & (t < nc + 3))
         def _():
             c = t - 3
-            for side in range(2):
-                x_copy(c, 6 + side).wait_recv()
+            settle(some(96), x_recv.at[c, 3])
             p_copy(c, 3).start()
-            for side in range(2):
-                x_copy(c, 2 + side).wait_recv()
+            settle(some(192), x_recv.at[c, 1])
             d_copy(c, core * nc + c, 0).start()
 
         @pl.when((t >= 4) & (t < nc + 4))
         def _():
             c = t - 4
-            for i in range(4):
-                p_copy(c, i).wait_recv()
+            settle(some(384), p_recv.at[c])
             d_copy(c, core * nc + c, 1).start()
             products(core * nc + c)
 
         @pl.when(t >= 5)
         def _():
             c = t - 5
-            for tensor in range(2):
-                d_copy(c, (1 - core) * nc + c, tensor).wait_recv()
+            settle(xc.at[0], d_recv.at[c])
             products((1 - core) * nc + c)
 
         return carry
@@ -336,7 +334,7 @@
 
     def e_copy(n, feature, c):
         if feature:
-            return remote(tps.at[c], tpr.at[c], e_send.at[n], e_recv.at[n], other_core)
+            return remote(s_f.at[c], tpr.at[c], e_send.at[n], e_recv.at[n], other_core)
         return remote(part_r, tpr_r, e_send.at[n], e_recv.at[n], other_core)
 
     def pick(feature, c, f_ref, r_ref):
@@ -346,28 +344,31 @@
         s, xa = pick(feature, c, s_f, s_r), pick(feature, c, xa_f, xa_r)
         at = pl.ds(((x + 2) % 4) * 192 + 96 * i, 96)
         return remote(
-            s.at[at], xa.at[i], a_send.at[n, i], a_recv.at[n, i], right if i == 0 else left
+            s.at[at], xa.at[i], a_send.at[int(feature)], a_recv.at[n], right if i == 0 else left
         )
 
     def b_copy(n, feature, c, i):
         s, xb = pick(feature, c, s_f, s_r), pick(feature, c, xb_f, xb_r)
         at = pl.ds(((x + 1 + 2 * i) % 4) * 192, 192)
         return remote(
-            s.at[at], xb.at[i], b_send.at[n, i], b_recv.at[n, i], right if i == 0 else left
+            s.at[at], xb.at[i], b_send.at[int(feature)], b_recv.at[n], right if i == 0 else left
         )
 
     def v_copy(n, feature, c, i):
         s, yr = pick(feature, c, s_f, s_r), pick(feature, c, yr_f, yr_r)
         at = pl.ds(block(x, y_peers[i]), BUNDLE)
         return remote(
-            s.at[at], yr.at[i], v_send.at[n, i], v_recv.at[n, i], chip(z, y_peers[i], x)
+            s.at[at], yr.at[i], v_send.at[int(feature)], v_recv.at[n], chip(z, y_peers[i], x)
         )
 
     def q_copy(n, feature, c, i):
         zs, zr = pick(feature, c, zs_f, zs_r), pick(feature, c, zr_f, zr_r)
         return remote(
-            zs.at[z_peers[i]], zr.at[i], q_send.at[n, i], q_recv.at[n, i], chip(z_peers[i], y, x)
-        )
+            zs.at[z_peers[i]], zr.at[i], q_send.at[int(feature)], q_recv.at[n], chip(z_peers[i], y, x)
+        )
+
+    def half_lanes(c):
+        return pl.ds(pl.multiple_of((c % 2) * LANES, LANES), LANES)
 
     def stage_core(n, feature, c):
         if not feature:
@@ -376,28 +377,28 @@
         k = (1 - core) * nc + c
         for m in range(3):
             rows = pl.ds(m * 256, 256)
-            tps[c, rows, :] = dot_nn(gsus[rows, :], wc[k]).astype(BF)
+            s_f[c, rows, :] = dot_nn(gsus[rows, :], wc[k]).astype(BF)
         e_copy(n, True, c).start()
         k = core * nc + c
         for m in range(3):
             rows = pl.ds(m * 256, 256)
-            part[c % 2, rows, :] = dot_nn(gsus[rows, :], wc[k])
+            pre[rows, half_lanes(c)] = dot_nn(gsus[rows, :], wc[k])
 
     def stage_a(n, feature, c):
-        e_copy(n, feature, c).wait_recv()
+        e_copy(n, feature, c).wait()
         s = pick(feature, c, s_f, s_r)
-        mine = part.at[c % 2] if feature else part_r
         theirs = pick(feature, c, tpr, tpr_r)
         for m in range(3):
             rows = pl.ds(m * 256, 256)
-            s[rows, :] = (mine[rows, :].astype(F32) + theirs[rows, :].astype(F32)).astype(BF)
+            mine = pre[rows, half_lanes(c)] if feature else part_r[rows, :].astype(F32)
+            s[rows, :] = (mine + theirs[rows, :].astype(F32)).astype(BF)
         for i in range(2):
             a_copy(n, feature, c, i).start()
 
     def stage_b(n, feature, c):
         s, xa = pick(feature, c, s_f, s_r), pick(feature, c, xa_f, xa_r)
+        settle(xa, a_recv.at[n])
         for i in range(2):
-            a_copy(n, feature, c, i).wait_recv()
             at = pl.ds(pl.multiple_of(((x + 1 + 2 * i) % 4) * 192 + 96 * i, 96), 96)
             s[at, :] = (s[at, :].astype(F32) + xa[i].astype(F32)).astype(BF)
         for i in range(2):
@@ -405,8 +406,7 @@
 
     def stage_v(n, feature, c):
         s, xb = pick(feature, c, s_f, s_r), pick(feature, c, xb_f, xb_r)
-        for i in range(2):
-            b_copy(n, feature, c, i).wait_recv()
+        settle(xb, b_recv.at[n])
         at = pl.ds(pl.multiple_of(x * 192, 192), 192)
         s[at, :] = (s[at, :].astype(F32) + xb[0].astype(F32) + xb[1].astype(F32)).astype(BF)
         for i in range(3):
@@ -415,8 +415,7 @@
     def stage_q(n, feature, c):
         s, yr = pick(feature, c, s_f, s_r), pick(feature, c, yr_f, yr_r)
         zs = pick(feature, c, zs_f, zs_r)
-        for i in range(3):
-            v_copy(n, feature, c, i).wait_recv()
+        settle(yr, v_recv.at[n])
         at = pl.ds(pl.multiple_of(block(x, y), BUNDLE), BUNDLE)
         mine = (s[at, :].astype(F32) + yr[0].astype(F32)).astype(BF)
         theirs = (yr[1].astype(F32) + yr[2].astype(F32)).astype(BF)
@@ -438,8 +437,7 @@
 
     def stage_out(n, feature, c):
         zs, zr = pick(feature, c, zs_f, zs_r), pick(feature, c, zr_f, zr_r)
-        for i in range(3):
-            q_copy(n, feature, c, i).wait_recv()
+        settle(zr, q_recv.at[n])
         total = zs[z].astype(F32)
         for i in range(3):
             total = total + zr[i].astype(F32)
@@ -452,9 +450,9 @@
     def out_copies(k):
         at = pl.ds(pl.multiple_of(k * LANES, LANES), LANES)
         return (
-            pltpu.make_async_copy(wc.at[k, pl.ds(0, hid)], out_gate.at[0, :, at], o_sem.at[k, 0]),
-            pltpu.make_async_copy(wc.at[k, pl.ds(SIDE_HID, hid)], out_up.at[0, :, at], o_sem.at[k, 1]),
-            pltpu.make_async_copy(wd.at[k], out_down.at[0, :, at], o_sem.at[k, 2]),
+            pltpu.make_async_copy(wc.at[k, pl.ds(0, hid)], out_gate.at[0, :, at], o_sem.at[0]),
+            pltpu.make_async_copy(wc.at[k, pl.ds(SIDE_HID, hid)], out_up.at[0, :, at], o_sem.at[1]),
+            pltpu.make_async_copy(wd.at[k], out_down.at[0, :, at], o_sem.at[2]),
         )
 
     def weight_grads(k):
@@ -488,47 +486,23 @@
 
     lax.fori_loop(0, nc + 1 + len(stages) - 1, give_back, 0)
 
-    for i in range(3):
-        zi_copy(i).wait_send()
-
-    def drain_dispatch(c, carry):
-        for i in range(3):
-            for tensor in range(2):
-                z_copy(c, i, tensor).wait_send()
-        for i in range(4):
-            y_copy(c, i).wait_send()
-            p_copy(c, i).wait_send()
-        for i in range(8):
-            x_copy(c, i).wait_send()
-        for tensor in range(2):
-            d_copy(c, core * nc + c, tensor).wait_send()
-        return carry
-
-    lax.fori_loop(0, nc, drain_dispatch, 0)
-
-    def drain_return(n, feature, c):
-        e_copy(n, feature, c).wait_send()
-        for i in range(2):
-            a_copy(n, feature, c, i).wait_send()
-            b_copy(n, feature, c, i).wait_send()
-        for i in range(3):
-            v_copy(n, feature, c, i).wait_send()
-            q_copy(n, feature, c, i).wait_send()
-
-    drain_return(0, False, 0)
-
-    def drain_features(n, carry):
-        drain_return(n, True, n - 1)
-        return carry
-
-    lax.fori_loop(1, nc + 1, drain_features, 0)
-
-    def drain_outputs(k, carry):
-        for cp in out_copies(k):
-            cp.wait()
-        return carry
-
-    lax.fori_loop(0, 2 * nc, drain_outputs, 0)
+    settle(iz.at[pl.ds(0, 3)], i_send.at[0])
+    settle(xc.at[0, :, pl.ds(0, 3 * rows_dev * nc)], z_send.at[0])
+    settle(xc.at[0], y_send.at[0])
+    settle(xc.at[pl.ds(0, 2)], x_send.at[0])
+    settle(xc.at[0], x_send.at[1])
+    settle(xc.at[0], x_send.at[2])
+    settle(xc.at[0, 0], x_send.at[3])
+    settle(xc.at[pl.ds(0, 2)], p_send.at[0])
+    settle(xc.at[pl.ds(0, nc)], d_send.at[0])
+    for sem, ref_r, ref_f in (
+        (a_send, xa_r, xa_f), (b_send, xb_r, xb_f), (v_send, yr_r, yr_f), (q_send, zr_r, zr_f)
+    ):
+        settle(ref_r, sem.at[0])
+        settle(ref_f, sem.at[1])
+    settle(out_gate.at[0], o_sem.at[0])
+    settle(out_up.at[0], o_sem.at[1])
+    settle(out_down.at[0], o_sem.at[2])
 
 
 def per_device(tokens, cotangent, routes, route_weights, gate_weight, up_weight, down_weight):
@@ -592,30 +566,28 @@
             vmem((slots, 2 * SIDE_HID), BF),
             vmem((2 * SIDE_HID, slots), BF),
             vmem((SIDE_HID, slots), BF),
-            vmem((2, slots, LANES), F32),
             vmem((nc, slots, LANES), BF),
             vmem((nc, slots, LANES), BF),
-            *chunk_buffers((nc,), LANES),
+            *chunk_buffers((nc,), LANES)[1:],
             vmem((slots, 128), BF),
             vmem((slots, 128), BF),
             *chunk_buffers((), 128),
-            dma((2 * nc, 3)),
-            dma((nc, 2)),
-            dma((nc, 3, 2)), dma((nc, 3, 2)),
-            dma((3,)), dma((3,)),
-            dma((nc, 4)), dma((nc, 4)),
-            dma((nc, 8)), dma((nc, 8)),
-            dma((nc, 4)), dma((nc, 4)),
-            dma((nc, 2)), dma((nc, 2)),
+            dma((3,)),
+            dma((1,)), dma((nc,)),
+            dma((1,)), dma((1,)),
+            dma((1,)), dma((nc, 2)),
+            dma((4,)), dma((nc, 4)),
+            dma((1,)), dma((nc,)),
+            dma((1,)), dma((nc,)),
             dma((nc + 1,)), dma((nc + 1,)),
-            dma((nc + 1, 2)), dma((nc + 1, 2)),
-            dma((nc + 1, 2)), dma((nc + 1, 2)),
-            dma((nc + 1, 3)), dma((nc + 1, 3)),
-            dma((nc + 1, 3)), dma((nc + 1, 3)),
-            dma((2 * nc, 3)),
+            dma((2,)), dma((nc + 1,)),
+            dma((2,)), dma((nc + 1,)),
+            dma((2,)), dma((nc + 1,)),
+            dma((2,)), dma((nc + 1,)),
+            dma((3,)),
         ],
         compiler_params=pltpu.CompilerParams(
-            collective_id=0, has_side_effects=True, vmem_limit_bytes=63 * 1024 * 1024
+            collective_id=0, has_side_effects=True, vmem_limit_bytes=43 * 1024 * 1024
         ),
     )(
         tokens, cotangent, routes.T, route_weights.T,

time: 129 us -> 120 us (0.930)
  Pallas kernels: 117 us -> 110 us
  local copies, waits for them, and re-layouts: 11 us -> 9.08 us
    pallas_call x1, Pallas kernels: 117 us -> 110 us  [per_device(): pl.pallas_call(functools.partial(kernel, nc, hid), out_shape=(jax.ShapeDt...]
    unnamed x9 -> x13, local copies, waits for them, and re-layouts: 11 us -> 9.08 us
where the time goes in v4:
time: 120 us
  Pallas kernels  110 us (92%)
  local copies, waits for them, and re-layouts  9.08 us (8%)
    pallas_call x1, Pallas kernels, per_device(): pl.pallas_call(functools.partial(kernel, nc, hid), out_shape=(jax.ShapeDt...  110 us
    unnamed x13, local copies, waits for them, and re-layouts  9.08 us

profile of v4, /device:TPU:0, one launch (start us, length us, event | category | flops | bytes accessed | tf_op | source)
XLA Modules:
  0.0 120.0 jit_solution(17124091987560532942)
XLA Ops:
  0.6 0.0 copy-start
  0.6 0.9 copy-done
  1.6 0.0 copy-start.1
  1.6 0.9 copy-done.1
  2.5 0.0 copy-start.2
  2.5 0.7 copy-done.2
  3.2 0.0 copy-start.3
  3.2 0.7 copy-done.3
  3.8 110.3 %shard_map.110 = (bf16[24,2048]{1,0:T(8,128)(2,1)S(1)}, f32[2,24]{1,0:T(2,128)S(1)}, bf16[1,344,4096]{2,1,0:T(8,128)(2,1)S(1)}, bf16[1,344,4096]{2,1,0:T(8,128)(2,1)S(1)}, bf16[1,344,4096]{2,1,0:T(8,128)(2,1)S(1)}) custom-call(bf16[24,4096]{1,0:T(8,128)(2,1)S(1)} %copy-done, bf16[24,4096]{1,0:T(8,128)(2,1)S(1)} %copy-done.1, s32[2,24]{1,0:T(2,128)S(1)} %bitcast.9, ...), custom_call_target="tpu_custom_call" | custom-call | tf_op jit(solution)/shard_map/pallas_call | solution.py:527
  114.1 0.6 copy.17
  114.8 0.6 copy.18
  115.3 1.6 %copy.19 = bf16[1,4096,344]{1,2,0:T(8,128)(2,1)} copy(bf16[1,4096,344]{1,2,0:T(8,128)(2,1)S(1)} %bitcast.8) | data formatting | bytes 5636096
  116.9 1.6 %copy.20 = bf16[1,4096,344]{1,2,0:T(8,128)(2,1)} copy(bf16[1,4096,344]{1,2,0:T(8,128)(2,1)S(1)} %bitcast.7) | data formatting | bytes 5636096
  118.4 1.6 %copy.21 = bf16[1,344,4096]{2,1,0:T(8,128)(2,1)} copy(bf16[1,344,4096]{2,1,0:T(8,128)(2,1)S(1)} %get-tuple-element.24) | data formatting | bytes 5636096
Async XLA Ops:
  0.6 0.9 copy-start
  1.6 0.9 copy-start.1
  2.5 0.7 copy-start.2
  3.2 0.7 copy-start.3

commit v5 on v4

--- a/solution.py
+++ b/solution.py
@@ -15,6 +15,9 @@
 BUNDLE = 48
 LANES = 256
 AHEAD = 3
+AT = (1, 2, 3, 4, 5)
+BACK_AT = (0, 1, 3, 5, 7, 9)
+GRADS_AT = 5
 SIDE_HID = 384
 BF = jnp.bfloat16
 F32 = jnp.float32
@@ -256,9 +259,9 @@
         def _():
             compact(t)
 
-        @pl.when((t >= 1) & (t < nc + 1))
-        def _():
-            c = t - 1
+        @pl.when((t >= AT[0]) & (t < nc + AT[0]))
+        def _():
+            c = t - AT[0]
             settle(some(BUNDLE), y_recv.at[c, 1])
             x_copy(c, 4).start()
             x_copy(c, 5).start()
@@ -273,9 +276,9 @@
             settle(up.at[0], w_sem.at[1])
             settle(down.at[0], w_sem.at[2])
 
-        @pl.when((t >= 2) & (t < nc + 2))
-        def _():
-            c = t - 2
+        @pl.when((t >= AT[1]) & (t < nc + AT[1]))
+        def _():
+            c = t - AT[1]
             settle(some(192), x_recv.at[c, 2])
             for side in range(2):
                 x_copy(c, 6 + side).start()
@@ -284,30 +287,30 @@
             for side in range(2):
                 x_copy(c, 2 + side).start()
 
-        @pl.when((t >= 3) & (t < nc + 3))
-        def _():
-            c = t - 3
+        @pl.when((t >= AT[2]) & (t < nc + AT[2]))
+        def _():
+            c = t - AT[2]
             settle(some(96), x_recv.at[c, 3])
             p_copy(c, 3).start()
             settle(some(192), x_recv.at[c, 1])
             d_copy(c, core * nc + c, 0).start()
 
-        @pl.when((t >= 4) & (t < nc + 4))
-        def _():
-            c = t - 4
+        @pl.when((t >= AT[3]) & (t < nc + AT[3]))
+        def _():
+            c = t - AT[3]
             settle(some(384), p_recv.at[c])
             d_copy(c, core * nc + c, 1).start()
             products(core * nc + c)
 
-        @pl.when(t >= 5)
-        def _():
-            c = t - 5
+        @pl.when(t >= AT[4])
+        def _():
+            c = t - AT[4]
             settle(xc.at[0], d_recv.at[c])
             products((1 - core) * nc + c)
 
         return carry
 
-    lax.fori_loop(0, nc + 5, dispatch, 0)
+    lax.fori_loop(0, nc + AT[4], dispatch, 0)
 
     def gates(m, carry):
         rows = pl.ds(pl.multiple_of(m * 128, 128), 128)
@@ -466,7 +469,7 @@
     stages = (stage_core, stage_a, stage_b, stage_v, stage_q, stage_out)
 
     def give_back(t, carry):
-        for depth, stage in enumerate(stages):
+        for depth, stage in zip(BACK_AT, stages):
             n = t - depth
 
             @pl.when(n == 0)
@@ -477,14 +480,14 @@
             def _():
                 stage(n, True, n - 1)
 
-        @pl.when((t >= 1) & (t <= nc))
-        def _():
-            weight_grads(core * nc + t - 1)
-            weight_grads((1 - core) * nc + t - 1)
+        @pl.when((t >= GRADS_AT) & (t < nc + GRADS_AT))
+        def _():
+            weight_grads(core * nc + t - GRADS_AT)
+            weight_grads((1 - core) * nc + t - GRADS_AT)
 
         return carry
 
-    lax.fori_loop(0, nc + 1 + len(stages) - 1, give_back, 0)
+    lax.fori_loop(0, nc + 1 + BACK_AT[-1], give_back, 0)
 
     settle(iz.at[pl.ds(0, 3)], i_send.at[0])
     settle(xc.at[0, :, pl.ds(0, 3 * rows_dev * nc)], z_send.at[0])

time: 120 us -> 113 us (0.942)
  Pallas kernels: 110 us -> 103 us
    pallas_call x1, Pallas kernels: 110 us -> 103 us  [per_device(): pl.pallas_call(functools.partial(kernel, nc, hid), out_shape=(jax.ShapeDt...]
where the time goes in v5:
time: 113 us
  Pallas kernels  103 us (91%)
  local copies, waits for them, and re-layouts  9.08 us (8%)
    pallas_call x1, Pallas kernels, per_device(): pl.pallas_call(functools.partial(kernel, nc, hid), out_shape=(jax.ShapeDt...  103 us
    unnamed x13, local copies, waits for them, and re-layouts  9.08 us

profile of v5, /device:TPU:0, one launch (start us, length us, event | category | flops | bytes accessed | tf_op | source)
XLA Modules:
  0.0 112.9 jit_solution(5656133157583432155)
XLA Ops:
  0.6 0.0 copy-start
  0.6 0.9 copy-done
  1.6 0.0 copy-start.1
  1.6 0.9 copy-done.1
  2.5 0.0 copy-start.2
  2.5 0.7 copy-done.2
  3.2 0.0 copy-start.3
  3.2 0.7 copy-done.3
  3.8 103.1 %shard_map.110 = (bf16[24,2048]{1,0:T(8,128)(2,1)S(1)}, f32[2,24]{1,0:T(2,128)S(1)}, bf16[1,344,4096]{2,1,0:T(8,128)(2,1)S(1)}, bf16[1,344,4096]{2,1,0:T(8,128)(2,1)S(1)}, bf16[1,344,4096]{2,1,0:T(8,128)(2,1)S(1)}) custom-call(bf16[24,4096]{1,0:T(8,128)(2,1)S(1)} %copy-done, bf16[24,4096]{1,0:T(8,128)(2,1)S(1)} %copy-done.1, s32[2,24]{1,0:T(2,128)S(1)} %bitcast.9, ...), custom_call_target="tpu_custom_call" | custom-call | tf_op jit(solution)/shard_map/pallas_call | solution.py:530
  107.0 0.6 copy.17
  107.6 0.6 copy.18
  108.2 1.6 %copy.19 = bf16[1,4096,344]{1,2,0:T(8,128)(2,1)} copy(bf16[1,4096,344]{1,2,0:T(8,128)(2,1)S(1)} %bitcast.8) | data formatting | bytes 5636096
  109.7 1.6 %copy.20 = bf16[1,4096,344]{1,2,0:T(8,128)(2,1)} copy(bf16[1,4096,344]{1,2,0:T(8,128)(2,1)S(1)} %bitcast.7) | data formatting | bytes 5636096
  111.3 1.6 %copy.21 = bf16[1,344,4096]{2,1,0:T(8,128)(2,1)} copy(bf16[1,344,4096]{2,1,0:T(8,128)(2,1)S(1)} %get-tuple-element.24) | data formatting | bytes 5636096
Async XLA Ops:
  0.6 0.9 copy-start
  1.6 0.9 copy-start.1
  2.5 0.7 copy-start.2
  3.2 0.7 copy-start.3

commit v6 on v5

--- a/solution.py
+++ b/solution.py
@@ -38,9 +38,9 @@
 
 def kernel(
     nc, hid,
-    tokens, cotangent, routes, weights, gate, up, down,
+    tokens, cotangent, routes_in, weights_in, gate, up, down,
     out_tok, out_rg, out_gate, out_up, out_down,
-    tz, info, iz, codes, xc, ob, place, place_t, share,
+    routes, weights, tz, info, iz, codes, xc, ob, place, firsts, place_t, share,
     wd, wc, pre, hg, gsus, gsus_t, hid_t,
     s_f, tpr, xa_f, xb_f, yr_f, zs_f, zr_f,
     part_r, tpr_r, s_r, xa_r, xb_r, yr_r, zs_r, zr_r,
@@ -71,6 +71,13 @@
     def block(xs, ys):
         return xs * 192 + (((ys + 1) // 2) % 2) * 96 + (ys // 2) * BUNDLE
 
+    small = [
+        pltpu.make_async_copy(routes_in, routes, w_sem.at[3]),
+        pltpu.make_async_copy(weights_in, weights, w_sem.at[4]),
+    ]
+    for cp in small:
+        cp.start()
+
     def pad_rows(c, carry):
         tz[c, :, :, rows_dev:, :] = jnp.zeros((SIDE, 2, ROWS - rows_dev, LANES), BF)
         return carry
@@ -96,8 +103,6 @@
     for cp in w_copies:
         cp.start()
 
-    pl.semaphore_wait(barrier, 9)
-
     def remote(a, b, ss, rs, dev):
         return pltpu.make_async_remote_copy(
             src_ref=a, dst_ref=b, send_sem=ss, recv_sem=rs, device_id=dev, device_id_type=MESH
@@ -135,8 +140,8 @@
                 z_copy(c, i, tensor).start()
             own_copy(c, tensor).start()
 
-    start_z(0)
-
+    for cp in small:
+        cp.wait()
     expert_row = lax.broadcasted_iota(jnp.int32, (EXPERTS, rows_dev), 0)
     hot = [expert_row == routes[k:k + 1, :] for k in range(2)]
     hit = jnp.where(hot[0] | hot[1], 1.0, 0.0).astype(BF)
@@ -152,13 +157,22 @@
     info[2, :, 0:rows_dev] = jnp.where(hot[0], weights[0:1, :], 0.0) + jnp.where(
         hot[1], weights[1:2, :], 0.0
     )
-    for i in range(3):
-        zi_copy(i).start()
-    for c in range(1, AHEAD):
-        start_z(c)
     iz[z] = info[...]
     pre[...] = jnp.zeros_like(pre)
     hg[...] = jnp.zeros_like(hg)
+
+    def blank(k, carry):
+        for at in (hid, SIDE_HID + hid):
+            wc[k, at:at + SIDE_HID - hid, :] = jnp.zeros((SIDE_HID - hid, LANES), BF)
+        return carry
+
+    lax.fori_loop(0, 2 * nc, blank, 0)
+
+    pl.semaphore_wait(barrier, 9)
+    for i in range(3):
+        zi_copy(i).start()
+    for c in range(AHEAD):
+        start_z(c)
     settle(iz.at[pl.ds(0, 3)], i_recv.at[0])
     for kind in range(3):
         total = iz[0, kind]
@@ -183,9 +197,7 @@
     first = jnp.concatenate(first + [spare], axis=0)
     second = jnp.concatenate(second + [spare], axis=0)
     place[...] = (first + second).astype(BF)
-    place_t[0] = (first + second).T.astype(BF)
-    place_t[1] = first.T.astype(BF)
-    place_t[2] = second.T.astype(BF)
+    firsts[...] = first
 
     def y_copy(c, i):
         k = core * nc + c
@@ -247,13 +259,6 @@
             pre[rows, :] += dot_nt(xc[k, 0, rows, :], wc[k])
             hg[rows, :hid] += dot_nt(xc[k, 1, rows, :], wd[k])
 
-    def blank(k, carry):
-        for at in (hid, SIDE_HID + hid):
-            wc[k, at:at + SIDE_HID - hid, :] = jnp.zeros((SIDE_HID - hid, LANES), BF)
-        return carry
-
-    lax.fori_loop(0, 2 * nc, blank, 0)
-
     def dispatch(t, carry):
         @pl.when(t < nc)
         def _():
@@ -311,6 +316,11 @@
         return carry
 
     lax.fori_loop(0, nc + AT[4], dispatch, 0)
+
+    first = firsts[...]
+    place_t[0] = place[...].astype(F32).T.astype(BF)
+    place_t[1] = first.T.astype(BF)
+    place_t[2] = (place[...].astype(F32) - first).T.astype(BF)
 
     def gates(m, carry):
         rows = pl.ds(pl.multiple_of(m * 128, 128), 128)
@@ -508,6 +518,33 @@
     settle(out_down.at[0], o_sem.at[2])
 
 
+def out_kernel(*refs):
+    count = (len(refs) - 1) // 2
+    sem = refs[-1]
+    copies = []
+    for i in range(count):
+        copies.append(pltpu.make_async_copy(refs[i], refs[count + i], sem.at[i]))
+    for cp in copies:
+        cp.start()
+    for cp in copies:
+        cp.wait()
+
+
+def in_hbm(a):
+    return pltpu.with_memory_space_constraint(a, pltpu.HBM)
+
+
+def put_out(*arrays):
+    return pl.pallas_call(
+        out_kernel,
+        out_shape=tuple(jax.ShapeDtypeStruct(a.shape, a.dtype) for a in arrays),
+        in_specs=[pl.BlockSpec(memory_space=pl.ANY)] * len(arrays),
+        out_specs=(pl.BlockSpec(memory_space=pl.ANY),) * len(arrays),
+        scratch_shapes=[pltpu.SemaphoreType.DMA((len(arrays),))],
+        compiler_params=pltpu.CompilerParams(vmem_limit_bytes=43 * 1024 * 1024),
+    )(*arrays)
+
+
 def per_device(tokens, cotangent, routes, route_weights, gate_weight, up_weight, down_weight):
     rows, width = tokens.shape
     half = width // lax.axis_size("tp")
@@ -539,8 +576,8 @@
         in_specs=[
             pl.BlockSpec(memory_space=anywhere),
             pl.BlockSpec(memory_space=anywhere),
-            pl.BlockSpec(memory_space=vmem),
-            pl.BlockSpec(memory_space=vmem),
+            pl.BlockSpec(memory_space=anywhere),
+            pl.BlockSpec(memory_space=anywhere),
             pl.BlockSpec(memory_space=anywhere),
             pl.BlockSpec(memory_space=anywhere),
             pl.BlockSpec(memory_space=anywhere),
@@ -553,6 +590,8 @@
             pl.BlockSpec(memory_space=anywhere),
         ),
         scratch_shapes=[
+            vmem((TOP, rows), jnp.int32),
+            vmem((TOP, rows), F32),
             vmem((nc, SIDE, 2, ROWS, LANES), BF),
             vmem((3, EXPERTS, 128), F32),
             vmem((SIDE, 3, EXPERTS, 128), F32),
@@ -560,6 +599,7 @@
             vmem((2 * nc, 2, slots, LANES), BF),
             vmem((nc, 2, BUNDLE, LANES), BF),
             vmem((128, 128), BF),
+            vmem((128, 128), F32),
             vmem((3, 128, 128), BF),
             vmem((2 * BUNDLE, 128), F32),
             vmem((2 * nc, hid, LANES), BF),
@@ -575,7 +615,7 @@
             vmem((slots, 128), BF),
             vmem((slots, 128), BF),
             *chunk_buffers((), 128),
-            dma((3,)),
+            dma((5,)),
             dma((1,)), dma((nc,)),
             dma((1,)), dma((1,)),
             dma((1,)), dma((nc, 2)),
@@ -593,8 +633,12 @@
             collective_id=0, has_side_effects=True, vmem_limit_bytes=43 * 1024 * 1024
         ),
     )(
-        tokens, cotangent, routes.T, route_weights.T,
-        gate_weight.transpose(0, 2, 1), up_weight.transpose(0, 2, 1), down_weight,
+        in_hbm(tokens), in_hbm(cotangent), in_hbm(routes.T), in_hbm(route_weights.T),
+        in_hbm(gate_weight.transpose(0, 2, 1)), in_hbm(up_weight.transpose(0, 2, 1)),
+        in_hbm(down_weight),
+    )
+    token_grad, shares, gate_grad, up_grad, down_grad = put_out(
+        token_grad, shares, gate_grad, up_grad, down_grad
     )
     return token_grad, shares.T, gate_grad.transpose(0, 2, 1), up_grad.transpose(0, 2, 1), down_grad
 

time: 113 us -> 107 us (0.947)
  local copies, waits for them, and re-layouts: 9.08 us -> 0 us
  Pallas kernels: 103 us -> 106 us
    unnamed x13 -> x0, local copies, waits for them, and re-layouts: 9.08 us -> none
    pallas_call x0 -> x1, Pallas kernels: none -> 3.49 us  [put_out(): pl.pallas_call(out_kernel, out_shape=tuple((jax.ShapeDtypeStruct(a.shape,...]
where the time goes in v6:
time: 107 us
  Pallas kernels  106 us (99%)
    pallas_call x1, Pallas kernels, per_device(): pl.pallas_call(functools.partial(kernel, nc, hid), out_shape=(jax.ShapeDt...  103 us
    pallas_call x1, Pallas kernels, put_out(): pl.pallas_call(out_kernel, out_shape=tuple((jax.ShapeDtypeStruct(a.shape,...  3.49 us

profile of v6, /device:TPU:0, one launch (start us, length us, event | category | flops | bytes accessed | tf_op | source)
XLA Modules:
  0.0 107.1 jit_solution(8823354763837585026)
XLA Ops:
  0.6 103.0 %shard_map.110 = (bf16[24,2048]{1,0:T(8,128)(2,1)S(1)}, f32[2,24]{1,0:T(2,128)S(1)}, bf16[1,344,4096]{2,1,0:T(8,128)(2,1)S(1)}, bf16[1,344,4096]{2,1,0:T(8,128)(2,1)S(1)}, bf16[1,344,4096]{2,1,0:T(8,128)(2,1)S(1)}) custom-call(bf16[24,4096]{1,0:T(8,128)(2,1)} %tokens.1, bf16[24,4096]{1,0:T(8,128)(2,1)} %cotangent.1, s32[2,24]{1,0:T(2,128)} %bitcast.9, ...), custom_call_target="tpu_custom_call" | custom-call | tf_op jit(solution)/shard_map/pallas_call | solution.py:567
  103.6 3.5 %shard_map.111 = (bf16[24,2048]{1,0:T(8,128)(2,1)}, f32[2,24]{1,0:T(2,128)}, bf16[1,344,4096]{2,1,0:T(8,128)(2,1)}, bf16[1,344,4096]{2,1,0:T(8,128)(2,1)}, bf16[1,344,4096]{2,1,0:T(8,128)(2,1)}) custom-call(bf16[24,2048]{1,0:T(8,128)(2,1)S(1)} %get-tuple-element.15.refs_0_, f32[2,24]{1,0:T(2,128)S(1)} %get-tuple-element.16.refs_1_, ...), custom_call_target="tpu_custom_call" | custom-call | tf_op jit(solution)/shard_map/pallas_call | solution.py:538

commit v7 on v6

--- a/solution.py
+++ b/solution.py
@@ -14,8 +14,8 @@
 ROWS = 32
 BUNDLE = 48
 LANES = 256
-AHEAD = 3
-AT = (1, 2, 3, 4, 5)
+AHEAD = 4
+AT = (2, 3, 4, 5, 6)
 BACK_AT = (0, 1, 3, 5, 7, 9)
 GRADS_AT = 5
 SIDE_HID = 384

time: 107 us -> 107 us (level)
  no operation moved by 1% of the time
where the time goes in v7:
time: 107 us
  Pallas kernels  106 us (99%)
    pallas_call x1, Pallas kernels, per_device(): pl.pallas_call(functools.partial(kernel, nc, hid), out_shape=(jax.ShapeDt...  102 us
    pallas_call x1, Pallas kernels, put_out(): pl.pallas_call(out_kernel, out_shape=tuple((jax.ShapeDtypeStruct(a.shape,...  3.49 us

profile of v7, /device:TPU:0, one launch (start us, length us, event | category | flops | bytes accessed | tf_op | source)
XLA Modules:
  0.0 106.6 jit_solution(3225146935100872348)
XLA Ops:
  0.6 102.5 %shard_map.110 = (bf16[24,2048]{1,0:T(8,128)(2,1)S(1)}, f32[2,24]{1,0:T(2,128)S(1)}, bf16[1,344,4096]{2,1,0:T(8,128)(2,1)S(1)}, bf16[1,344,4096]{2,1,0:T(8,128)(2,1)S(1)}, bf16[1,344,4096]{2,1,0:T(8,128)(2,1)S(1)}) custom-call(bf16[24,4096]{1,0:T(8,128)(2,1)} %tokens.1, bf16[24,4096]{1,0:T(8,128)(2,1)} %cotangent.1, s32[2,24]{1,0:T(2,128)} %bitcast.9, ...), custom_call_target="tpu_custom_call" | custom-call | tf_op jit(solution)/shard_map/pallas_call | solution.py:567
  103.1 3.5 %shard_map.111 = (bf16[24,2048]{1,0:T(8,128)(2,1)}, f32[2,24]{1,0:T(2,128)}, bf16[1,344,4096]{2,1,0:T(8,128)(2,1)}, bf16[1,344,4096]{2,1,0:T(8,128)(2,1)}, bf16[1,344,4096]{2,1,0:T(8,128)(2,1)}) custom-call(bf16[24,2048]{1,0:T(8,128)(2,1)S(1)} %get-tuple-element.15.refs_0_, f32[2,24]{1,0:T(2,128)S(1)} %get-tuple-element.16.refs_1_, ...), custom_call_target="tpu_custom_call" | custom-call | tf_op jit(solution)/shard_map/pallas_call | solution.py:538

commit v8 on v7

--- a/solution.py
+++ b/solution.py
@@ -317,11 +317,6 @@
 
     lax.fori_loop(0, nc + AT[4], dispatch, 0)
 
-    first = firsts[...]
-    place_t[0] = place[...].astype(F32).T.astype(BF)
-    place_t[1] = first.T.astype(BF)
-    place_t[2] = (place[...].astype(F32) - first).T.astype(BF)
-
     def gates(m, carry):
         rows = pl.ds(pl.multiple_of(m * 128, 128), 128)
         value = jnp.zeros((128, 1), F32)
@@ -489,6 +484,13 @@
             @pl.when((n >= 1) & (n <= nc))
             def _():
                 stage(n, True, n - 1)
+
+        @pl.when(t == 2)
+        def _():
+            first = firsts[...]
+            place_t[0] = place[...].astype(F32).T.astype(BF)
+            place_t[1] = first.T.astype(BF)
+            place_t[2] = (place[...].astype(F32) - first).T.astype(BF)
 
         @pl.when((t >= GRADS_AT) & (t < nc + GRADS_AT))
         def _():

time: 107 us -> 107 us (level)
  no operation moved by 1% of the time
where the time goes in v8:
time: 107 us
  Pallas kernels  106 us (99%)
    pallas_call x1, Pallas kernels, per_device(): pl.pallas_call(functools.partial(kernel, nc, hid), out_shape=(jax.ShapeDt...  102 us
    pallas_call x1, Pallas kernels, put_out(): pl.pallas_call(out_kernel, out_shape=tuple((jax.ShapeDtypeStruct(a.shape,...  3.49 us

profile of v8, /device:TPU:0, one launch (start us, length us, event | category | flops | bytes accessed | tf_op | source)
XLA Modules:
  0.0 106.6 jit_solution(553504859773167367)
XLA Ops:
  0.6 102.5 %shard_map.110 = (bf16[24,2048]{1,0:T(8,128)(2,1)S(1)}, f32[2,24]{1,0:T(2,128)S(1)}, bf16[1,344,4096]{2,1,0:T(8,128)(2,1)S(1)}, bf16[1,344,4096]{2,1,0:T(8,128)(2,1)S(1)}, bf16[1,344,4096]{2,1,0:T(8,128)(2,1)S(1)}) custom-call(bf16[24,4096]{1,0:T(8,128)(2,1)} %tokens.1, bf16[24,4096]{1,0:T(8,128)(2,1)} %cotangent.1, s32[2,24]{1,0:T(2,128)} %bitcast.9, ...), custom_call_target="tpu_custom_call" | custom-call | tf_op jit(solution)/shard_map/pallas_call | solution.py:569
  103.1 3.5 %shard_map.111 = (bf16[24,2048]{1,0:T(8,128)(2,1)}, f32[2,24]{1,0:T(2,128)}, bf16[1,344,4096]{2,1,0:T(8,128)(2,1)}, bf16[1,344,4096]{2,1,0:T(8,128)(2,1)}, bf16[1,344,4096]{2,1,0:T(8,128)(2,1)}) custom-call(bf16[24,2048]{1,0:T(8,128)(2,1)S(1)} %get-tuple-element.15.refs_0_, f32[2,24]{1,0:T(2,128)S(1)} %get-tuple-element.16.refs_1_, ...), custom_call_target="tpu_custom_call" | custom-call | tf_op jit(solution)/shard_map/pallas_call | solution.py:540
